TPU v7x, 128 devices: a whole 4x4x4 slice. The times are simulated.
128 devices in a mesh: sp: 64 (over z, y, x), tp: 2 (over core).
Axes of the slice: x: 4, y: 4, z: 4, core: 2. Of those that a mesh axis runs over, the one named last changes fastest.
Arguments:
- resid: bfloat16 [16384, 2048], P(('sp', 'tp')), may hold values from -6 to 6
- value_in: bfloat16 [16384, 1536], P('sp', 'tp'), may hold values from -6 to 6
- gate_in: bfloat16 [16384, 1536], P('sp', 'tp'), may hold values from -8 to 8
- conv_weight: float32 [31, 1536], P(None, 'tp'), may hold values from -2.5 to 2.5
- norm_gain: float32 [1536], P('tp'), may hold values from 0.1 to 1.9
- out_weight: bfloat16 [1536, 2048], replicated, may hold values from -0.15625 to 0.15625
- ffn_gain: float32 [2048], replicated, may hold values from 0.1 to 1.9
- expert_ids: int32 [16384, 2], P(('sp', 'tp')), may hold values from 0 to 127, all different within a row; in each aligned block of 128 rows (0 to 127, 128 to 255, ...) at most 4 rows name the same one
- expert_mix: float32 [16384, 2], P(('sp', 'tp')), may hold values from 0.1 to 1
- w_gate: bfloat16 [128, 2048, 1024], P(('sp', 'tp')), may hold values from -0.125 to 0.125
- w_up: bfloat16 [128, 2048, 1024], P(('sp', 'tp')), may hold values from -0.125 to 0.125
- w_down: bfloat16 [128, 1024, 2048], P(('sp', 'tp')), may hold values from -0.1875 to 0.1875
Outputs:
- layer_out: bfloat16 [16384, 2048], P(('sp', 'tp'))
Inputs may be any that keep to these rules, and one draw needn't show every extreme that they name: `expert_ids`: each row names 2 different experts; within each aligned block of 128 rows no expert is named by more than 4 rows, a bound that some block reaches.
All inputs are finite; a program needn't handle non-finite values.
Results may differ from a plain program's by a relative error of at most 0.012.
Values may be sent and summed in bfloat16 or wider, within the bound.
A program may use at most 128 MiB of HBM per device.

v0:
```python
import jax
import jax.numpy as jnp
from jax import lax
from jax.sharding import PartitionSpec as P


def padded_2(block, sides, width):
    for axis, dim in sides:
        count = lax.axis_size(axis)
        forward = [(i, i + 1) for i in range(count - 1)]
        backward = [(target, source) for source, target in forward]
        low = lax.ppermute(
            lax.slice_in_dim(block, block.shape[dim] - width, None, axis=dim), axis, forward
        )
        high = lax.ppermute(lax.slice_in_dim(block, 0, width, axis=dim), axis, backward)
        block = jnp.concatenate([low, block, high], axis=dim)
    return block


def expert_apply(rows, gate_w, up_w, down_w):
    gate = jnp.dot(rows, gate_w, preferred_element_type=jnp.float32)
    up = jnp.dot(rows, up_w, preferred_element_type=jnp.float32)
    hidden = (jax.nn.silu(gate) * up).astype(jnp.bfloat16)
    return jnp.dot(hidden, down_w, preferred_element_type=jnp.float32).astype(jnp.bfloat16)


def per_device(
    resid,
    value_in,
    gate_in,
    conv_weight,
    norm_gain,
    out_weight,
    ffn_gain,
    expert_ids,
    expert_mix,
    w_gate,
    w_up,
    w_down,
):
    glu = (value_in.astype(jnp.float32) * jax.nn.sigmoid(gate_in.astype(jnp.float32))).astype(
        jnp.bfloat16
    )
    taps = conv_weight.shape[0]
    reach = taps // 2
    length = glu.shape[0]
    local_width = glu.shape[1]
    padded = padded_2(glu, (("sp", 0),), reach).astype(jnp.float32)
    conv = jnp.zeros((length, local_width), jnp.float32)
    for tap in range(taps):
        conv = conv + padded[tap : tap + length] * conv_weight[tap]
    sums = lax.psum((jnp.sum(conv, axis=1), jnp.sum(conv * conv, axis=1)), "tp")
    width = local_width * lax.axis_size("tp")
    mean = sums[0] / width
    var = sums[1] / width - mean * mean
    normed_conv = (conv - mean[:, None]) * lax.rsqrt(var + 1e-05)[:, None] * norm_gain
    mixed = jax.nn.silu(normed_conv).astype(jnp.bfloat16)
    regrouped = lax.all_to_all(mixed, "tp", split_axis=0, concat_axis=1, tiled=True)
    proj = jnp.dot(regrouped, out_weight, preferred_element_type=jnp.float32)
    stream = (resid.astype(jnp.float32) + proj).astype(jnp.bfloat16)
    wide = stream.astype(jnp.float32)
    normed = (
        wide * lax.rsqrt(jnp.mean(wide * wide, axis=1, keepdims=True) + 1e-06) * ffn_gain
    ).astype(jnp.bfloat16)
    sp_count = lax.axis_size("sp")
    tp_count = lax.axis_size("tp")
    experts_all = sp_count * tp_count
    rows_here = stream.shape[0]
    topk = expert_ids.shape[1]
    model_width = stream.shape[1]
    cap = max(2, (2 * topk * rows_here + experts_all - 1) // experts_all)
    flat = expert_ids.reshape(-1)
    onehot = (flat[:, None] == jnp.arange(experts_all, dtype=jnp.int32)[None, :]).astype(jnp.int32)
    rank = jnp.sum(jnp.cumsum(onehot, axis=0) * onehot, axis=1) - 1
    dest = flat * cap + rank
    owner = jnp.arange(rows_here * topk, dtype=jnp.int32) // topk
    table = jnp.full((experts_all * cap,), rows_here, jnp.int32).at[dest].set(owner)
    source = jnp.concatenate([normed, jnp.zeros((1, model_width), jnp.bfloat16)], axis=0)
    outgoing = jnp.take(source, table, axis=0).reshape(experts_all, cap, model_width)
    gate_w, up_w, down_w = (w_gate[0], w_up[0], w_down[0])
    arrived = lax.all_to_all(outgoing, ("sp", "tp"), split_axis=0, concat_axis=0, tiled=True)
    shape = arrived.shape
    done = expert_apply(arrived.reshape(-1, model_width), gate_w, up_w, down_w).reshape(shape)
    returned = lax.all_to_all(done, ("sp", "tp"), split_axis=0, concat_axis=0, tiled=True)
    picked = jnp.take(returned.reshape(experts_all * cap, model_width), dest, axis=0)
    picked = picked.astype(jnp.float32).reshape(rows_here, topk, model_width)
    total = wide + jnp.sum(picked * expert_mix[:, :, None], axis=1)
    return total.astype(jnp.bfloat16)


def solution(mesh):
    return jax.shard_map(
        per_device,
        mesh=mesh,
        in_specs=(
            P(("sp", "tp"), None),
            P("sp", "tp"),
            P("sp", "tp"),
            P(None, "tp"),
            P("tp"),
            P(),
            P(),
            P(("sp", "tp"), None),
            P(("sp", "tp"), None),
            P(("sp", "tp"), None, None),
            P(("sp", "tp"), None, None),
            P(("sp", "tp"), None, None),
        ),
        out_specs=P(("sp", "tp"), None),
        check_vma=False,
    )
```

profile of v0, /device:TPU:1, one launch (start us, length us, event | category | flops | bytes accessed | tf_op | source)
XLA Modules:
  0.0 148.9 jit_solution(16317060824717870948)
XLA Ops:
  0.0 1.3 multiply_convert_fusion.3
  1.4 3.9 %collective-permute-start = (bf16[15,768]{1,0:T(8,128)(2,1)S(1)}, bf16[15,768]{1,0:T(8,128)(2,1)S(1)}, u32[]{:S(2)}, u32[]{:S(2)}) collective-permute-start(bf16[15,768]{1,0:T(8,128)(2,1)S(1)} %get-tuple-element.41), channel_id=1, source_target_pairs={{0,2},{2,4},{4,6},{6,8},{8,10},{10,12},{12,14},{14,16},{16,18},{18... | collective-permute-start | bytes 69128 | tf_op jit(solution)/shard_map/ppermute | solution.py:12
  5.3 1.3 collective-permute-start.1
  6.6 1.5 slice_reduce_fusion.30
  8.1 1.2 slice_reduce_fusion.29
  9.3 0.8 copy.29
  10.1 0.1 eq.26
  10.2 0.1 reshape.106
  10.3 0.7 broadcast_multiply_fusion
  11.0 0.1 copy.31
  11.1 0.2 fusion.45
  11.5 0.2 fusion.46
  11.6 0.1 copy.35
  11.8 0.1 mul.499
  11.9 1.4 scatter_custom_fusion
  13.4 0.1 broadcast_in_dim.38
  13.5 0.0 collective-permute-done
  13.5 0.0 collective-permute-done.1
  13.5 0.1 maximum_convert_fusion
  13.6 0.0 copy-start.4
  13.6 4.2 %fusion.52 = (f32[256]{0:T(256)S(1)}, f32[256]{0:T(256)S(1)}, f32[256,768]{1,0:T(8,128)S(1)}) fusion(f32[768]{0:T(1024)S(1)} %get-tuple-element.36, f32[286,768]{1,0:T(8,128)S(1)} %maximum_convert_fusion, f32[768]{0:T(1024)S(1)} %get-tuple-element.37, f32[768]{0:T(1024)S(1)} %get-tuple-element.8, f32[768]{0:T(1024)S(1)} %get-tuple-element.9, ...), kind=kLoop, calls=%fused_computation.144 | loop fusion | flops 12582400 | bytes 25263104 | tf_op jit(solution)/shard_map/reduce_sum | solution.py:52
  17.8 0.0 copy-start.1
  17.8 3.2 %all-reduce.1 = (f32[256]{0:T(256)S(1)}, f32[256]{0:T(256)S(1)}) all-reduce(f32[256]{0:T(256)S(1)} %get-tuple-element.6, f32[256]{0:T(256)S(1)} %get-tuple-element.5), channel_id=1, replica_groups=mesh['sp'=64,'tp'=2] {'tp'}, use_global_device_ids=true, to_apply=%region_3.0 | all-reduce | flops 512 | bytes 4096 | tf_op jit(solution)/shard_map/psum | solution.py:52
  21.0 0.0 copy-done.4
  21.0 0.3 multiply_convert_fusion.2
  21.4 4.0 %all_to_all.29 = bf16[2,128,768]{2,1,0:T(8,128)(2,1)S(1)} all-to-all(bf16[2,128,768]{2,1,0:T(8,128)(2,1)S(1)} %bitcast.37), channel_id=1, replica_groups=mesh['sp'=64,'tp'=2] {'tp'}, dimensions={0} | all-to-all | bytes 786432 | tf_op jit(solution)/shard_map/all_to_all | solution.py:58
  25.4 0.2 copy.28
  25.6 0.0 copy-done.1
  25.6 0.0 copy-start.3
  25.6 3.9 %multiply_reduce_fusion.1 = (f32[128]{0:T(128)S(1)}, f32[128,2048]{1,0:T(8,128)S(1)}) fusion(bf16[128,1536]{0,1:T(8,128)(2,1)S(1)} %bitcast.35, bf16[1536,2048]{1,0:T(8,128)(2,1)} %param.17, bf16[128,2048]{1,0:T(8,128)(2,1)S(1)} %copy-done.1), kind=kOutput, calls=%fused_computation.19 | convolution fusion | flops 806879104 | bytes 8258048 | tf_op jit(solution)/shard_map/dot_general | solution.py:59
  29.5 0.0 copy-done.3
  29.5 0.2 multiply_convert_fusion.1
  29.7 3.3 %gather_fusion = bf16[512,2048]{1,0:T(8,128)(2,1)} fusion(bf16[129,2048]{1,0:T(8,128)(2,1)S(1)} %concatenate.7, s32[1024]{0:T(1024)S(1)} %pad_clamp_fusion.1), kind=kCustom, calls=%fused_computation | custom fusion | bytes 4196352 | tf_op jit(solution)/shard_map/jit(_take)/gather | solution.py:79
  33.1 2.7 %gather.13 = bf16[128,4,2048]{2,1,0:T(4,128)(2,1)S(1)} reshape(bf16[512,2048]{1,0:T(8,128)(2,1)} %gather_fusion) | data formatting | bytes 4194304 | tf_op jit(solution)/shard_map/jit(_take)/gather | solution.py:79
  35.8 1.0 broadcast_select_fusion
  36.9 41.8 %all_to_all.30 = bf16[128,4,2048]{2,1,0:T(4,128)(2,1)S(1)} all-to-all(bf16[128,4,2048]{2,1,0:T(4,128)(2,1)S(1)} %broadcast_select_fusion), channel_id=1, replica_groups=mesh['sp'=64,'tp'=2] {'sp','tp'}, dimensions={0} | all-to-all | bytes 4194304 | tf_op jit(solution)/shard_map/all_to_all | solution.py:81
  78.7 2.0 %reshape.108 = bf16[512,2048]{1,0:T(8,128)(2,1)} reshape(bf16[128,4,2048]{2,1,0:T(4,128)(2,1)S(1)} %all_to_all.30) | data formatting | bytes 4194304 | tf_op jit(solution)/shard_map/reshape | solution.py:83
  80.7 0.0 copy-start
  80.7 6.6 %fusion.4 = f32[512,1024]{1,0:T(8,128)} fusion(bf16[512,2048]{1,0:T(8,128)(2,1)} %reshape.108, bf16[1,2048,1024]{2,1,0:T(8,128)(2,1)} %param.21), kind=kOutput, calls=%fused_computation.7 | convolution fusion | flops 2147483648 | bytes 8388608 | tf_op jit(solution)/shard_map/dot_general | solution.py:21
  87.3 0.0 copy-done
  87.3 9.9 %fusion.6 = bf16[512,2048]{1,0:T(8,128)(2,1)} fusion(bf16[1,1024,2048]{2,1,0:T(8,128)(2,1)} %param.23, f32[512,1024]{1,0:T(8,128)} %fusion.4, bf16[512,2048]{1,0:T(8,128)(2,1)S(1)} %copy-done, bf16[1,2048,1024]{2,1,0:T(8,128)(2,1)} %param.22), kind=kOutput, calls=%fused_computation.9 | convolution fusion | flops 4299161600 | bytes 14680064 | tf_op jit(solution)/shard_map/dot_general | solution.py:24
  97.2 4.1 %reshape.109 = bf16[128,4,2048]{2,1,0:T(4,128)(2,1)} reshape(bf16[512,2048]{1,0:T(8,128)(2,1)} %fusion.6) | data formatting | bytes 4194304 | tf_op jit(solution)/shard_map/reshape | solution.py:83
  101.4 0.0 copy-start.2
  101.4 0.0 copy-start.5
  101.4 5.6 %all-to-all-start.2 = ((bf16[128,4,2048]{2,1,0:T(4,128)(2,1)}), bf16[128,4,2048]{2,1,0:T(4,128)(2,1)}, u32[]{:S(2)}, u32[]{:S(2)}) async-start(bf16[128,4,2048]{2,1,0:T(4,128)(2,1)} %reshape.109), calls=%async_computation.2 | async-start | bytes 4194304 | tf_op jit(solution)/shard_map/all_to_all | solution.py:84
  107.0 0.1 sub.29
  107.1 0.1 copy.33
  107.2 0.0 copy-done.2
  107.2 0.1 copy.34
  107.3 0.0 copy-done.5
  107.3 0.1 copy.36
  107.5 29.7 %all-to-all-done.2 = bf16[128,4,2048]{2,1,0:T(4,128)(2,1)} async-done(((bf16[128,4,2048]{2,1,0:T(4,128)(2,1)}), bf16[128,4,2048]{2,1,0:T(4,128)(2,1)}, u32[]{:S(2)}, u32[]{:S(2)}) %all-to-all-start.2) | async-done | bytes 2097184 | tf_op jit(solution)/shard_map/all_to_all | solution.py:84
  137.2 2.5 %reshape.110 = bf16[512,2048]{1,0:T(8,128)(2,1)S(1)} reshape(bf16[128,4,2048]{2,1,0:T(4,128)(2,1)} %all-to-all-done.2) | data formatting | bytes 4194304 | tf_op jit(solution)/shard_map/reshape | solution.py:85
  139.7 2.3 %gather_fusion.1 = bf16[256,2048]{1,0:T(8,128)(2,1)} fusion(bf16[512,2048]{1,0:T(8,128)(2,1)S(1)} %reshape.110, s32[1024]{0:T(1024)S(1)} %pad_clamp_fusion), kind=kCustom, calls=%fused_computation.1 | custom fusion | bytes 2098176 | tf_op jit(solution)/shard_map/jit(_take)/gather | solution.py:85
  142.1 1.7 %gather.15 = bf16[128,2,2048]{2,1,0:T(2,128)(2,1)S(1)} reshape(bf16[256,2048]{1,0:T(8,128)(2,1)} %gather_fusion.1) | data formatting | bytes 2097152 | tf_op jit(solution)/shard_map/jit(_take)/gather | solution.py:85
  143.8 4.1 %multiply_reduce_fusion = f32[128,2048]{1,0:T(8,128)S(1)} fusion(bf16[128,2,2048]{2,1,0:T(2,128)(2,1)S(1)} %gather.15, pred[128,2]{1,0:T(8,128)(4,1)S(1)} %copy.34, f32[128,2]{1,0:T(8,128)S(1)} %copy.36), kind=kLoop, calls=%fused_computation.13 | loop fusion | flops 1835008 | bytes 2098432 | tf_op jit(solution)/shard_map/reduce_sum | solution.py:87
  147.9 0.9 add_convert_fusion
  (18 shorter events, 0.2 us)
Async XLA Ops:
  1.4 12.1 %collective-permute-start = (bf16[15,768]{1,0:T(8,128)(2,1)S(1)}, bf16[15,768]{1,0:T(8,128)(2,1)S(1)}, u32[]{:S(2)}, u32[]{:S(2)}) collective-permute-start(bf16[15,768]{1,0:T(8,128)(2,1)S(1)} %get-tuple-element.41), channel_id=1, source_target_pairs={{0,2},{2,4},{4,6},{6,8},{8,10},{10,12},{12,14},{14,16},{16,18},{18... | collective-permute-start | bytes 69128 | tf_op jit(solution)/shard_map/ppermute | solution.py:12
  5.3 8.2 %collective-permute-start.1 = (bf16[15,768]{1,0:T(8,128)(2,1)S(1)}, bf16[15,768]{1,0:T(8,128)(2,1)S(1)}, u32[]{:S(2)}, u32[]{:S(2)}) collective-permute-start(bf16[15,768]{1,0:T(8,128)(2,1)S(1)} %get-tuple-element.42), channel_id=1, source_target_pairs={{2,0},{4,2},{6,4},{8,6},{10,8},{12,10},{14,12},{16,14},{18,16},{20... | collective-permute-start | bytes 69128 | tf_op jit(solution)/shard_map/ppermute | solution.py:15
  13.6 7.4 %copy-start.4 = (f32[768]{0:T(1024)S(1)}, f32[768]{0:T(1024)}, u32[]{:S(2)}) copy-start(f32[768]{0:T(1024)} %param.16) | copy-start | bytes 9220
  17.8 7.8 %copy-start.1 = (bf16[128,2048]{1,0:T(8,128)(2,1)S(1)}, bf16[128,2048]{1,0:T(8,128)(2,1)}, u32[]{:S(2)}) copy-start(bf16[128,2048]{1,0:T(8,128)(2,1)} %param.12) | copy-start | bytes 1572868
  25.6 3.9 %copy-start.3 = (f32[2048]{0:T(1024)S(1)}, f32[2048]{0:T(1024)}, u32[]{:S(2)}) copy-start(f32[2048]{0:T(1024)} %param.18) | copy-start | bytes 24580
  80.7 6.7 %copy-start = (bf16[512,2048]{1,0:T(8,128)(2,1)S(1)}, bf16[512,2048]{1,0:T(8,128)(2,1)}, u32[]{:S(2)}) copy-start(bf16[512,2048]{1,0:T(8,128)(2,1)} %reshape.108) | copy-start | bytes 6291460
  101.4 5.8 %copy-start.2 = (s32[128,2]{0,1:T(2,128)S(1)}, s32[128,2]{0,1:T(2,128)}, u32[]{:S(2)}) copy-start(s32[128,2]{0,1:T(2,128)} %param.19) | copy-start | bytes 3076
  101.4 6.0 %copy-start.5 = (f32[128,2]{0,1:T(2,128)S(1)}, f32[128,2]{0,1:T(2,128)}, u32[]{:S(2)}) copy-start(f32[128,2]{0,1:T(2,128)} %param.20) | copy-start | bytes 3076
  101.4 35.8 %all-to-all-start.2 = ((bf16[128,4,2048]{2,1,0:T(4,128)(2,1)}), bf16[128,4,2048]{2,1,0:T(4,128)(2,1)}, u32[]{:S(2)}, u32[]{:S(2)}) async-start(bf16[128,4,2048]{2,1,0:T(4,128)(2,1)} %reshape.109), calls=%async_computation.2 | async-start | bytes 4194304 | tf_op jit(solution)/shard_map/all_to_all | solution.py:84
where the time goes:
time: 150 us; the launch traced here: 149 us
  blocking collectives  49 us (33%)
  waiting for transfers between devices  29.7 us (20%)
  local copies, waits for them, and re-layouts  25.2 us (17%)
  matrix products  20.4 us (14%)
  other arithmetic  13.3 us (9%)
  starting transfers between devices  10.8 us (7%)
    all_to_all x1, blocking collectives, per_device(): lax.all_to_all(outgoing, ('sp', 'tp'), split_axis=0, concat_axis=0, tiled...  41.8 us
    all_to_all x1, waiting for transfers between devices, per_device(): lax.all_to_all(done, ('sp', 'tp'), split_axis=0, concat_axis=0, tiled=True)  29.7 us
    dot_general x1, matrix products, expert_apply(): jnp.dot(hidden, down_w, preferred_element_type=jnp.float32)  9.9 us
    dot_general x1, matrix products, expert_apply(): gate = jnp.dot(rows, gate_w, preferred_element_type=jnp.float32)  6.65 us
    gather x2, local copies, waits for them, and re-layouts, per_device(): jnp.take(source, table, axis=0).reshape(experts_all, cap, model_width)  6.08 us
    all_to_all x1, starting transfers between devices, per_device(): lax.all_to_all(done, ('sp', 'tp'), split_axis=0, concat_axis=0, tiled=True)  5.59 us
    reduce_sum x1, other arithmetic, per_device(): sums = lax.psum((jnp.sum(conv, axis=1), jnp.sum(conv * conv, axis=1)), 'tp')  4.16 us
    reshape x1, local copies, waits for them, and re-layouts, per_device(): expert_apply(arrived.reshape(-1, model_width), gate_w, up_w, down_w)  4.11 us
  transfers between devices with their start and end apart: 3, of which 1 were waited for; matrix products, arithmetic and copies ran while one was open for 5% of the time, Pallas kernels for 0%

commit v1 on v0

v1 whole, which is shorter than its diff:
```python
import functools

import jax
import jax.numpy as jnp
from jax import lax
from jax.experimental import pallas as pl
from jax.experimental.pallas import tpu as pltpu
from jax.sharding import PartitionSpec as P

MESH = pl.DeviceIdType.MESH
BF = jnp.bfloat16
F32 = jnp.float32
CAP = 4
N = 128
HALF = 64
TILE = 512


def padded_2(block, sides, width):
    for axis, dim in sides:
        count = lax.axis_size(axis)
        forward = [(i, i + 1) for i in range(count - 1)]
        backward = [(target, source) for source, target in forward]
        low = lax.ppermute(
            lax.slice_in_dim(block, block.shape[dim] - width, None, axis=dim), axis, forward
        )
        high = lax.ppermute(lax.slice_in_dim(block, 0, width, axis=dim), axis, backward)
        block = jnp.concatenate([low, block, high], axis=dim)
    return block


def offsets(i):
    a, b, c = i % 4, (i // 4) % 4, (i // 16) % 4
    return a, (a + b) % 4, (a + b + c) % 4, i // 64


def device_at(i, sign):
    sp, tp = lax.axis_index("sp"), lax.axis_index("tp")
    dz, dy, dx, dc = offsets(i)
    z, y, x = sp // 16, (sp // 4) % 4, sp % 4
    z, y, x = (z + 4 + sign * dz) % 4, (y + 4 + sign * dy) % 4, (x + 4 + sign * dx) % 4
    return (z * 4 + y) * 4 + x, (tp + dc) % 2


def moe_kernel(
    normed_ref, stream_ref, ids_ref, mix_ref, wg_hbm, wu_hbm, wd_hbm,
    out_ref,
    wg, wu, wd, sendbuf, recvbuf, ysend, yrecv, xs, hid, gates, wt_hi, wt_lo, acc,
    wsem, dsend, drecv, rsend, rrecv,
):
    sp, tp = lax.axis_index("sp"), lax.axis_index("tp")
    weights = [
        pltpu.make_async_copy(wg_hbm, wg, wsem.at[0]),
        pltpu.make_async_copy(wu_hbm, wu, wsem.at[1]),
        pltpu.make_async_copy(wd_hbm, wd, wsem.at[2]),
    ]
    for copy in weights:
        copy.start()
    barrier = pltpu.get_barrier_semaphore()

    def greet(i, carry):
        pl.semaphore_signal(barrier, inc=1, device_id=device_at(i, 1), device_id_type=MESH)
        return carry

    lax.fori_loop(1, N, greet, 0)

    slot = lax.broadcasted_iota(jnp.int32, (N, CAP * N), 1)
    i, r = slot // CAP, slot % CAP
    dz, dy, dx, dc = offsets(i)
    z, y, x = (sp // 16 + dz) % 4, ((sp // 4) % 4 + dy) % 4, (sp % 4 + dx) % 4
    expert = ((z * 4 + y) * 4 + x) * 2 + (tp + dc) % 2
    first = ids_ref[:, 0:1] == expert
    second = ids_ref[:, 1:2] == expert
    named = jnp.where(first | second, 1.0, 0.0)
    rows = lax.broadcasted_iota(jnp.int32, (N, N), 0)
    cols = lax.broadcasted_iota(jnp.int32, (N, N), 1)
    before = jnp.where(cols < rows, 1.0, 0.0).astype(BF)
    rank = jnp.dot(before, named.astype(BF), preferred_element_type=F32)
    chosen = jnp.where(rank == r.astype(F32), named, 0.0)
    gates[...] = jnp.transpose(chosen).astype(BF)
    weight = chosen * jnp.where(first, mix_ref[:, 0:1], mix_ref[:, 1:2])
    high = weight.astype(BF)
    wt_hi[...] = high
    wt_lo[...] = (weight - high.astype(F32)).astype(BF)

    def fill(g, carry):
        lhs = gates[pl.ds(pl.multiple_of(g * 128, 128), 128), :]
        for k in range(4):
            part = jnp.dot(
                lhs, normed_ref[:, k * TILE:(k + 1) * TILE], preferred_element_type=F32
            ).astype(BF)
            sendbuf[pl.ds(g * 32, 32), :, k * TILE:(k + 1) * TILE] = part.reshape(32, CAP, TILE)
        return carry

    lax.fori_loop(0, 4, fill, 0)
    recvbuf[0] = sendbuf[0]
    pl.semaphore_wait(barrier, N - 1)

    def dispatch(chunk):
        def one(i, carry):
            pltpu.make_async_remote_copy(
                src_ref=sendbuf.at[i], dst_ref=recvbuf.at[i],
                send_sem=dsend, recv_sem=drecv.at[chunk],
                device_id=device_at(i, 1), device_id_type=MESH,
            ).start()
            return carry

        lax.fori_loop(max(1, chunk * HALF), (chunk + 1) * HALF, one, 0)

    def giveback(chunk):
        def one(i, carry):
            pltpu.make_async_remote_copy(
                src_ref=ysend.at[i], dst_ref=yrecv.at[i],
                send_sem=rsend, recv_sem=rrecv.at[chunk],
                device_id=device_at(i, -1), device_id_type=MESH,
            ).start()
            return carry

        lax.fori_loop(max(1, chunk * HALF), (chunk + 1) * HALF, one, 0)

    def whole(chunk, source, target, send, recv):
        low = max(1, chunk * HALF)
        span = pl.ds(low, (chunk + 1) * HALF - low)
        return pltpu.make_async_remote_copy(
            src_ref=source.at[span], dst_ref=target.at[span], send_sem=send,
            recv_sem=recv.at[chunk], device_id=device_at(1, 1), device_id_type=MESH,
        )

    dispatch(0)
    dispatch(1)
    rows_chunk = HALF * CAP
    for chunk in range(2):
        whole(chunk, sendbuf, recvbuf, dsend, drecv).wait_recv()
        if chunk == 0:
            for copy in weights:
                copy.wait()

        def gather(g, carry):
            span = pl.ds(pl.multiple_of(g * 64, 64), 64)
            xs[span, :] = recvbuf[pl.ds(chunk * HALF + g * 16, 16)].reshape(64, 2048)
            return carry

        lax.fori_loop(0, 4, gather, 0)

        def up(j, carry):
            col = pl.ds(pl.multiple_of(j * TILE, TILE), TILE)
            gate = jnp.dot(xs[...], wg[:, col], preferred_element_type=F32)
            value = jnp.dot(xs[...], wu[:, col], preferred_element_type=F32)
            hid[:, col] = (gate * jax.nn.sigmoid(gate) * value).astype(BF)
            return carry

        lax.fori_loop(0, 1024 // TILE, up, 0)

        def down(j, carry):
            col = pl.ds(pl.multiple_of(j * TILE, TILE), TILE)
            part = jnp.dot(hid[...], wd[:, col], preferred_element_type=F32).astype(BF)
            ysend[chunk * HALF:(chunk + 1) * HALF, :, col] = part.reshape(HALF, CAP, TILE)
            return carry

        lax.fori_loop(0, 2048 // TILE, down, 0)
        if chunk == 0:
            yrecv[0] = ysend[0]
        giveback(chunk)

    for chunk in range(2):
        whole(chunk, ysend, yrecv, rsend, rrecv).wait_recv()
        slots = slice(chunk * rows_chunk, (chunk + 1) * rows_chunk)
        lhs_hi, lhs_lo = wt_hi[:, slots], wt_lo[:, slots]

        def combine(j, carry):
            col = pl.ds(pl.multiple_of(j * TILE, TILE), TILE)
            got = yrecv[chunk * HALF:(chunk + 1) * HALF, :, col].reshape(rows_chunk, TILE)
            part = jnp.dot(lhs_hi, got, preferred_element_type=F32)
            part = part + jnp.dot(lhs_lo, got, preferred_element_type=F32)
            if chunk == 0:
                acc[:, col] = part + stream_ref[:, col].astype(F32)
            else:
                out_ref[:, col] = (acc[:, col] + part).astype(BF)
            return carry

        lax.fori_loop(0, 2048 // TILE, combine, 0)
    for chunk in range(2):
        whole(chunk, sendbuf, recvbuf, dsend, drecv).wait_send()
        whole(chunk, ysend, yrecv, rsend, rrecv).wait_send()


def moe(normed, stream, ids, mix, w_gate, w_up, w_down):
    vmem = pl.BlockSpec(memory_space=pltpu.VMEM)
    hbm = pl.BlockSpec(memory_space=pltpu.HBM)
    slots = pltpu.VMEM((N, CAP, 2048), BF)
    return pl.pallas_call(
        moe_kernel,
        out_shape=jax.ShapeDtypeStruct((N, 2048), BF),
        in_specs=[vmem, vmem, vmem, vmem, hbm, hbm, hbm],
        out_specs=vmem,
        scratch_shapes=[
            pltpu.VMEM((2048, 1024), BF),
            pltpu.VMEM((2048, 1024), BF),
            pltpu.VMEM((1024, 2048), BF),
            slots, slots, slots, slots,
            pltpu.VMEM((HALF * CAP, 2048), BF),
            pltpu.VMEM((HALF * CAP, 1024), BF),
            pltpu.VMEM((CAP * N, N), BF),
            pltpu.VMEM((N, CAP * N), BF),
            pltpu.VMEM((N, CAP * N), BF),
            pltpu.VMEM((N, 2048), F32),
            pltpu.SemaphoreType.DMA((3,)),
            pltpu.SemaphoreType.DMA,
            pltpu.SemaphoreType.DMA((2,)),
            pltpu.SemaphoreType.DMA,
            pltpu.SemaphoreType.DMA((2,)),
        ],
        compiler_params=pltpu.CompilerParams(
            collective_id=0, has_side_effects=True, vmem_limit_bytes=56 * 2**20
        ),
        name="moe",
    )(normed, stream, ids, mix, w_gate, w_up, w_down)


def per_device(
    resid,
    value_in,
    gate_in,
    conv_weight,
    norm_gain,
    out_weight,
    ffn_gain,
    expert_ids,
    expert_mix,
    w_gate,
    w_up,
    w_down,
):
    glu = (value_in.astype(F32) * jax.nn.sigmoid(gate_in.astype(F32))).astype(BF)
    taps = conv_weight.shape[0]
    reach = taps // 2
    length = glu.shape[0]
    local_width = glu.shape[1]
    padded = padded_2(glu, (("sp", 0),), reach).astype(F32)
    conv = jnp.zeros((length, local_width), F32)
    for tap in range(taps):
        conv = conv + padded[tap : tap + length] * conv_weight[tap]
    sums = lax.psum((jnp.sum(conv, axis=1), jnp.sum(conv * conv, axis=1)), "tp")
    width = local_width * lax.axis_size("tp")
    mean = sums[0] / width
    var = sums[1] / width - mean * mean
    normed_conv = (conv - mean[:, None]) * lax.rsqrt(var + 1e-05)[:, None] * norm_gain
    mixed = jax.nn.silu(normed_conv).astype(BF)
    regrouped = lax.all_to_all(mixed, "tp", split_axis=0, concat_axis=1, tiled=True)
    proj = jnp.dot(regrouped, out_weight, preferred_element_type=F32)
    stream = (resid.astype(F32) + proj).astype(BF)
    wide = stream.astype(F32)
    normed = (
        wide * lax.rsqrt(jnp.mean(wide * wide, axis=1, keepdims=True) + 1e-06) * ffn_gain
    ).astype(BF)
    return moe(normed, stream, expert_ids, expert_mix, w_gate[0], w_up[0], w_down[0])


def solution(mesh):
    return jax.shard_map(
        per_device,
        mesh=mesh,
        in_specs=(
            P(("sp", "tp"), None),
            P("sp", "tp"),
            P("sp", "tp"),
            P(None, "tp"),
            P("tp"),
            P(),
            P(),
            P(("sp", "tp"), None),
            P(("sp", "tp"), None),
            P(("sp", "tp"), None, None),
            P(("sp", "tp"), None, None),
            P(("sp", "tp"), None, None),
        ),
        out_specs=P(("sp", "tp"), None),
        check_vma=False,
    )
```

time: 150 us -> 101 us (0.67)
  Pallas kernels: 0 us -> 69.7 us
  blocking collectives: 49 us -> 7.1 us
  waiting for transfers between devices: 29.7 us -> 0.01 us
  local copies, waits for them, and re-layouts: 25.2 us -> 7.55 us
  matrix products: 20.4 us -> 3.9 us
  other arithmetic: 13.3 us -> 6.92 us
  starting transfers between devices: 10.8 us -> 5.23 us
    pallas_call x0 -> x1, Pallas kernels: none -> 69.7 us  [moe(): pl.pallas_call(moe_kernel, out_shape=jax.ShapeDtypeStruct((N, 2048), BF),...]
    all_to_all x1 -> x0, blocking collectives: 41.8 us -> none  [per_device(): lax.all_to_all(outgoing, ('sp', 'tp'), split_axis=0, concat_axis=0, tiled...]
    all_to_all x1 -> x0, waiting for transfers between devices: 29.7 us -> none  [per_device(): lax.all_to_all(done, ('sp', 'tp'), split_axis=0, concat_axis=0, tiled=True)]
    dot_general x3 -> x1, matrix products: 20.4 us -> 3.9 us  [per_device(): proj = jnp.dot(regrouped, out_weight, preferred_element_type=F32)]
    gather x4 -> x0, local copies, waits for them, and re-layouts: 10.2 us -> none  [the longest x2 6.08 us: per_device(): jnp.take(source, table, axis=0).reshape(experts_all, cap, model_width)]
    reshape x4 -> x0, local copies, waits for them, and re-layouts: 8.82 us -> none  [the longest x1 4.11 us: per_device(): expert_apply(arrived.reshape(-1, model_width), gate_w, up_w, down_w)]
    all_to_all x1 -> x0, starting transfers between devices: 5.59 us -> none  [per_device(): lax.all_to_all(done, ('sp', 'tp'), split_axis=0, concat_axis=0, tiled=True)]
    reduce_sum x2 -> x0, other arithmetic: 4.25 us -> none  [the longest x1 4.07 us: per_device(): total = wide + jnp.sum(picked * expert_mix[:, :, None], axis=1)]
  transfers between devices with their start and end apart: 3 -> 2, of which waited for: 1 -> 0; matrix products, arithmetic and copies ran while one was open for 5% -> 5% of each run, Pallas kernels for 0% -> 0%
where the time goes in v1:
time: 101 us
  Pallas kernels  69.7 us (69%)
  local copies, waits for them, and re-layouts  7.55 us (7%)
  blocking collectives  7.1 us (7%)
  other arithmetic  6.92 us (7%)
  starting transfers between devices  5.23 us (5%)
  matrix products  3.9 us (4%)
    pallas_call x1, Pallas kernels, moe(): pl.pallas_call(moe_kernel, out_shape=jax.ShapeDtypeStruct((N, 2048), BF),...  69.7 us
    unnamed x11, local copies, waits for them, and re-layouts  4.71 us
    reduce_sum x1, other arithmetic, per_device(): sums = lax.psum((jnp.sum(conv, axis=1), jnp.sum(conv * conv, axis=1)), 'tp')  4.16 us
    all_to_all x1, blocking collectives, per_device(): lax.all_to_all(mixed, 'tp', split_axis=0, concat_axis=1, tiled=True)  4.02 us
    ppermute x1, starting transfers between devices, padded_2(): lax.ppermute(lax.slice_in_dim(block, block.shape[dim] - width, None, axis...  3.93 us
    dot_general x1, matrix products, per_device(): proj = jnp.dot(regrouped, out_weight, preferred_element_type=F32)  3.9 us
    psum x1, blocking collectives, per_device(): sums = lax.psum((jnp.sum(conv, axis=1), jnp.sum(conv * conv, axis=1)), 'tp')  3.08 us
    slice x2, local copies, waits for them, and re-layouts, per_device(): conv = conv + padded[tap:tap + length] * conv_weight[tap]  2.62 us
  transfers between devices with their start and end apart: 2, of which 0 were waited for; matrix products, arithmetic and copies ran while one was open for 5% of the time, Pallas kernels for 0%

profile of v1, /device:TPU:1, one launch (start us, length us, event | category | flops | bytes accessed | tf_op | source)
XLA Modules:
  0.0 100.5 jit_solution(13470641208454684655)
XLA Ops:
  0.0 1.3 %multiply_convert_fusion.1 = bf16[256,768]{1,0:T(8,128)(2,1)S(1)} fusion(bf16[256,768]{1,0:T(8,128)(2,1)} %param.14, bf16[256,768]{1,0:T(8,128)(2,1)} %param.13), kind=kLoop, calls=%fused_computation.70 | loop fusion | flops 1376256 | bytes 1179648 | tf_op jit(solution)/shard_map/convert_element_type | solution.py:234
  1.4 3.9 %collective-permute-start = (bf16[15,768]{1,0:T(8,128)(2,1)S(1)}, bf16[15,768]{1,0:T(8,128)(2,1)S(1)}, u32[]{:S(2)}, u32[]{:S(2)}) collective-permute-start(bf16[15,768]{1,0:T(8,128)(2,1)S(1)} %get-tuple-element.41), channel_id=1, source_target_pairs={{0,2},{2,4},{4,6},{6,8},{8,10},{10,12},{12,14},{14,16},{16,18},{18... | collective-permute-start | bytes 69128 | tf_op jit(solution)/shard_map/ppermute | solution.py:24
  5.3 1.3 %collective-permute-start.1 = (bf16[15,768]{1,0:T(8,128)(2,1)S(1)}, bf16[15,768]{1,0:T(8,128)(2,1)S(1)}, u32[]{:S(2)}, u32[]{:S(2)}) collective-permute-start(bf16[15,768]{1,0:T(8,128)(2,1)S(1)} %get-tuple-element.42), channel_id=1, source_target_pairs={{2,0},{4,2},{6,4},{8,6},{10,8},{12,10},{14,12},{16,14},{18,16},{20... | collective-permute-start | bytes 69128 | tf_op jit(solution)/shard_map/ppermute | solution.py:27
  6.6 1.5 %slice_reduce_fusion.30 = (f32[768]{0:T(1024)S(1)}, f32[768]{0:T(1024)S(1)}, f32[768]{0:T(1024)S(1)}, f32[768]{0:T(1024)S(1)}, f32[768]{0:T(1024)S(1)}, /*index=...) fusion(f32[31,768]{1,0:T(8,128)} %param.15), kind=kLoop, calls=%fused_computation.102 | loop fusion | bytes 116736 | tf_op jit(solution)/shard_map/slice | solution.py:242
  8.1 1.1 %slice_reduce_fusion.29 = (f32[768]{0:T(1024)S(1)}, f32[768]{0:T(1024)S(1)}, f32[768]{0:T(1024)S(1)}, f32[768]{0:T(1024)S(1)}, f32[768]{0:T(1024)S(1)}, /*index=...) fusion(f32[31,768]{1,0:T(8,128)} %param.15), kind=kLoop, calls=%fused_computation.101 | loop fusion | bytes 73728 | tf_op jit(solution)/shard_map/slice | solution.py:242
  9.2 1.4 %copy.18.ids_ref = s32[128,2]{1,0:T(8,128)} copy(s32[128,2]{0,1:T(2,128)} %param.19) | data formatting | bytes 2048 | tf_op args[7]
  10.6 1.4 %copy.19.mix_ref = f32[128,2]{1,0:T(8,128)} copy(f32[128,2]{0,1:T(2,128)} %param.20) | data formatting | bytes 2048 | tf_op args[8]
  12.0 0.0 collective-permute-done
  12.0 0.0 collective-permute-done.1
  12.0 0.1 maximum_convert_fusion
  12.1 0.0 copy-start.3
  12.1 0.0 copy-start.1
  12.2 4.2 %fusion.34 = (f32[256]{0:T(256)S(1)}, f32[256]{0:T(256)S(1)}, f32[256,768]{1,0:T(8,128)S(1)}) fusion(f32[768]{0:T(1024)S(1)} %get-tuple-element.36, f32[286,768]{1,0:T(8,128)S(1)} %maximum_convert_fusion, f32[768]{0:T(1024)S(1)} %get-tuple-element.37, f32[768]{0:T(1024)S(1)} %get-tuple-element.8, f32[768]{0:T(1024)S(1)} %get-tuple-element.9, ...), kind=kLoop, calls=%fused_computation.106 | loop fusion | flops 12582400 | bytes 25263104 | tf_op jit(solution)/shard_map/reduce_sum | solution.py:243
  16.3 3.1 %all-reduce = (f32[256]{0:T(256)S(1)}, f32[256]{0:T(256)S(1)}) all-reduce(f32[256]{0:T(256)S(1)} %get-tuple-element.6, f32[256]{0:T(256)S(1)} %get-tuple-element.5), channel_id=1, replica_groups=mesh['sp'=64,'tp'=2] {'tp'}, use_global_device_ids=true, to_apply=%region_3.0 | all-reduce | flops 512 | bytes 4096 | tf_op jit(solution)/shard_map/psum | solution.py:243
  19.4 0.0 copy-done.3
  19.4 0.3 multiply_convert_fusion
  19.8 4.0 %all_to_all.19 = bf16[2,128,768]{2,1,0:T(8,128)(2,1)S(1)} all-to-all(bf16[2,128,768]{2,1,0:T(8,128)(2,1)S(1)} %bitcast.13), channel_id=1, replica_groups=mesh['sp'=64,'tp'=2] {'tp'}, dimensions={0} | all-to-all | bytes 786432 | tf_op jit(solution)/shard_map/all_to_all | solution.py:249
  23.8 0.2 copy.17
  24.0 0.0 copy-done.1
  24.0 0.0 copy-start.2
  24.0 3.9 %fusion.1 = (f32[128]{0:T(128)S(1)}, bf16[128,2048]{1,0:T(8,128)(2,1)S(1)}) fusion(bf16[128,1536]{0,1:T(8,128)(2,1)S(1)} %bitcast.11, bf16[1536,2048]{1,0:T(8,128)(2,1)} %param.17, bf16[128,2048]{1,0:T(8,128)(2,1)S(1)} %copy-done.1), kind=kOutput, calls=%fused_computation.4 | convolution fusion | flops 806879104 | bytes 7733760 | tf_op jit(solution)/shard_map/dot_general | solution.py:250
  27.9 0.0 copy-start
  27.9 0.0 copy-done.2
  28.0 1.0 fusion.3.normed_ref
  28.9 0.0 copy-done
  28.9 69.7 %moe.1 = bf16[128,2048]{1,0:T(8,128)(2,1)} custom-call(bf16[128,2048]{1,0:T(8,128)(2,1)} %fusion.3.normed_ref, bf16[128,2048]{1,0:T(8,128)(2,1)} %copy-done, s32[128,2]{1,0:T(8,128)} %copy.18.ids_ref, f32[128,2]{1,0:T(8,128)} %copy.19.mix_ref, bf16[2048,1024]{1,0:T(8,128)(2,1)} %bitcast.8, bf16[2048,1024]{1,0:T(8,128)(2,1)} %bitcast.9, ...), custom_call_target="tpu_custom_call" | custom-call | tf_op jit(solution)/shard_map/moe/pallas_call | solution.py:191
  98.7 1.9 %copy.21 = bf16[128,2048]{1,0:T(8,128)(2,1)} copy(bf16[128,2048]{1,0:T(8,128)(2,1)} %moe.1) | data formatting | bytes 1048576
  (3 shorter events, 0.0 us)
Async XLA Ops:
  1.4 10.7 %collective-permute-start = (bf16[15,768]{1,0:T(8,128)(2,1)S(1)}, bf16[15,768]{1,0:T(8,128)(2,1)S(1)}, u32[]{:S(2)}, u32[]{:S(2)}) collective-permute-start(bf16[15,768]{1,0:T(8,128)(2,1)S(1)} %get-tuple-element.41), channel_id=1, source_target_pairs={{0,2},{2,4},{4,6},{6,8},{8,10},{10,12},{12,14},{14,16},{16,18},{18... | collective-permute-start | bytes 69128 | tf_op jit(solution)/shard_map/ppermute | solution.py:24
  5.3 6.7 %collective-permute-start.1 = (bf16[15,768]{1,0:T(8,128)(2,1)S(1)}, bf16[15,768]{1,0:T(8,128)(2,1)S(1)}, u32[]{:S(2)}, u32[]{:S(2)}) collective-permute-start(bf16[15,768]{1,0:T(8,128)(2,1)S(1)} %get-tuple-element.42), channel_id=1, source_target_pairs={{2,0},{4,2},{6,4},{8,6},{10,8},{12,10},{14,12},{16,14},{18,16},{20... | collective-permute-start | bytes 69128 | tf_op jit(solution)/shard_map/ppermute | solution.py:27
  12.1 7.3 %copy-start.3 = (f32[768]{0:T(1024)S(1)}, f32[768]{0:T(1024)}, u32[]{:S(2)}) copy-start(f32[768]{0:T(1024)} %param.16) | copy-start | bytes 9220
  12.1 11.9 %copy-start.1 = (bf16[128,2048]{1,0:T(8,128)(2,1)S(1)}, bf16[128,2048]{1,0:T(8,128)(2,1)}, u32[]{:S(2)}) copy-start(bf16[128,2048]{1,0:T(8,128)(2,1)} %param.12) | copy-start | bytes 1572868
  24.0 3.9 %copy-start.2 = (f32[2048]{0:T(1024)S(1)}, f32[2048]{0:T(1024)}, u32[]{:S(2)}) copy-start(f32[2048]{0:T(1024)} %param.18) | copy-start | bytes 24580
  27.9 1.0 %copy-start = (bf16[128,2048]{1,0:T(8,128)(2,1)}, bf16[128,2048]{1,0:T(8,128)(2,1)S(1)}, u32[]{:S(2)}) copy-start(bf16[128,2048]{1,0:T(8,128)(2,1)S(1)} %get-tuple-element.46.stream_ref) | copy-start | bytes 1572868

commit v2 on v1

v2 whole, which is shorter than its diff:
```python
import functools

import jax
import jax.numpy as jnp
from jax import lax
from jax.experimental import pallas as pl
from jax.experimental.pallas import tpu as pltpu
from jax.sharding import PartitionSpec as P

MESH = pl.DeviceIdType.MESH
BF = jnp.bfloat16
F32 = jnp.float32
CAP = 4
N = 128
HALF = 64
TILE = 512


def offsets(i):
    a, b, c = i % 4, (i // 4) % 4, (i // 16) % 4
    return a, (a + b) % 4, (a + b + c) % 4, i // 64


def device_at(i, sign):
    sp, tp = lax.axis_index("sp"), lax.axis_index("tp")
    dz, dy, dx, dc = offsets(i)
    z, y, x = sp // 16, (sp // 4) % 4, sp % 4
    z, y, x = (z + 4 + sign * dz) % 4, (y + 4 + sign * dy) % 4, (x + 4 + sign * dx) % 4
    return (z * 4 + y) * 4 + x, (tp + dc) % 2


def device_in_line(dz, dy, dx, dc):
    sp, tp = lax.axis_index("sp"), lax.axis_index("tp")
    z, y, x = (sp // 16 + dz) % 4, ((sp // 4) % 4 + dy) % 4, (sp % 4 + dx) % 4
    return (z * 4 + y) * 4 + x, (tp + dc) % 2


def layer_kernel(
    resid_hbm, value_ref, gate_ref, taps_in, gain_in, ow_hbm, ffn_gain_ref, ids_ref, mix_ref,
    wg_hbm, wu_hbm, wd_hbm,
    out_ref,
    wg, wu, wd, ow, resid, taps, taps_other, gain_other, glu, other, halo, padded, conv, mixed, stream, normed,
    sendbuf, recvbuf, ysend, yrecv, xs, hid, gates, wt_hi, wt_lo, acc,
    wsem, tsend, trecv, gsend, grecv, hsend, hrecv, dsend, drecv, rsend, rrecv, y_ready, z_ready,
):
    sp, tp = lax.axis_index("sp"), lax.axis_index("tp")
    barrier = pltpu.get_barrier_semaphore()

    def signal(semaphore, device):
        pl.semaphore_signal(semaphore, inc=1, device_id=device, device_id_type=MESH)

    for dc in range(2):
        for dx in range(4):
            if dx or dc:
                signal(barrier, device_in_line(0, 0, dx, dc))
    for step in range(1, 4):
        signal(barrier, device_in_line(0, step, 0, 0))
        signal(barrier, device_in_line(step, 0, 0, 0))
    halo_from = jnp.where(tp == 0, sp - 1, sp + 1)
    has_halo = (halo_from >= 0) & (halo_from < 64)

    @pl.when(has_halo)
    def _():
        signal(barrier, (halo_from, 0))
        signal(barrier, (halo_from, 1))

    resid_copy = pltpu.make_async_copy(resid_hbm, resid, wsem.at[0])
    ow_copy = pltpu.make_async_copy(ow_hbm, ow, wsem.at[1])
    weights = [
        pltpu.make_async_copy(wg_hbm, wg, wsem.at[2]),
        pltpu.make_async_copy(wu_hbm, wu, wsem.at[3]),
        pltpu.make_async_copy(wd_hbm, wd, wsem.at[4]),
    ]
    for copy in [ow_copy, resid_copy] + weights:
        copy.start()

    def gated(g, carry):
        span = pl.ds(pl.multiple_of(g * 32, 32), 32)
        value = value_ref[span, :].astype(F32)
        glu[span, :] = (value * jax.nn.sigmoid(gate_ref[span, :].astype(F32))).astype(BF)
        return carry

    lax.fori_loop(0, 8, gated, 0)
    expected = 13 + jnp.where(sp > 0, 1, 0) + jnp.where(sp < 63, 1, 0)
    pl.semaphore_wait(barrier, expected)

    peer_rows = pl.ds(pl.multiple_of(112 * (1 - tp), 16), 144)
    to_peer = pltpu.make_async_remote_copy(
        src_ref=glu.at[peer_rows], dst_ref=other, send_sem=gsend, recv_sem=grecv,
        device_id=(sp, 1 - tp), device_id_type=MESH,
    )
    to_peer.start()
    taps_to_peer = pltpu.make_async_remote_copy(
        src_ref=taps_in, dst_ref=taps_other, send_sem=tsend.at[0], recv_sem=trecv.at[0],
        device_id=(sp, 1 - tp), device_id_type=MESH,
    )
    taps_to_peer.start()
    gain_to_peer = pltpu.make_async_remote_copy(
        src_ref=gain_in, dst_ref=gain_other, send_sem=tsend.at[1], recv_sem=trecv.at[1],
        device_id=(sp, 1 - tp), device_id_type=MESH,
    )
    gain_to_peer.start()
    to_next = pltpu.make_async_remote_copy(
        src_ref=glu.at[pl.ds(240, 16)], dst_ref=halo.at[tp], send_sem=hsend.at[0],
        recv_sem=hrecv.at[tp], device_id=(sp + 1, 0), device_id_type=MESH,
    )
    to_previous = pltpu.make_async_remote_copy(
        src_ref=glu.at[pl.ds(0, 16)], dst_ref=halo.at[tp], send_sem=hsend.at[1],
        recv_sem=hrecv.at[tp], device_id=(sp - 1, 1), device_id_type=MESH,
    )

    @pl.when(sp < 63)
    def _():
        to_next.start()

    @pl.when(sp > 0)
    def _():
        to_previous.start()

    for step in range(1, 4):
        signal(y_ready, device_in_line(0, step, 0, 0))

    own_rows = pl.multiple_of(112 * tp, 16)
    inner = pl.multiple_of(16 * (1 - tp), 16)
    edge = pl.multiple_of(144 * tp, 16)
    edge_out = pl.multiple_of(112 * tp, 16)
    for k in range(6):
        lanes = slice(k * 128, (k + 1) * 128)
        padded[tp * 6 + k, pl.ds(inner, 144), :] = glu[pl.ds(own_rows, 144), lanes].astype(F32)
        taps[tp * 6 + k, 0:31, :] = taps_in[:, lanes]
        taps[tp * 6 + k, 31:32, :] = gain_in[lanes].reshape(1, 128)

    def convolve(block, start, count):
        total = jnp.zeros((count, 128), F32)
        for tap in range(31):
            total = total + padded[block, pl.ds(start + tap + 1, count), :] * taps[block, tap:tap + 1, :]
        conv[block, pl.ds(start, count), :] = total

    def inner_blocks(first):
        def one(k, carry):
            convolve(first + k, inner, 56)
            convolve(first + k, inner + 56, 56)
            return carry

        lax.fori_loop(0, 6, one, 0)

    inner_blocks(tp * 6)
    to_peer.wait_recv()
    taps_to_peer.wait_recv()
    gain_to_peer.wait_recv()
    for k in range(6):
        lanes = slice(k * 128, (k + 1) * 128)
        padded[(1 - tp) * 6 + k, pl.ds(inner, 144), :] = other[:, lanes].astype(F32)
        taps[(1 - tp) * 6 + k, 0:31, :] = taps_other[:, lanes]
        taps[(1 - tp) * 6 + k, 31:32, :] = gain_other[lanes].reshape(1, 128)
    pl.semaphore_wait(y_ready, 3)
    for step in range(1, 4):
        signal(z_ready, device_in_line(step, 0, 0, 0))
    inner_blocks((1 - tp) * 6)

    @pl.when(has_halo)
    def _():
        for c in range(2):
            pltpu.make_async_remote_copy(
                src_ref=glu.at[pl.ds(0, 16)], dst_ref=halo.at[c], send_sem=hsend.at[0],
                recv_sem=hrecv.at[c], device_id=(sp, 1 - tp), device_id_type=MESH,
            ).wait_recv()
            for k in range(6):
                lanes = slice(k * 128, (k + 1) * 128)
                padded[c * 6 + k, pl.ds(edge, 16), :] = halo[c, :, lanes].astype(F32)

    @pl.when(jnp.logical_not(has_halo))
    def _():
        for k in range(12):
            padded[k, pl.ds(edge, 16), :] = jnp.zeros((16, 128), F32)

    def edges(k, carry):
        convolve(k, edge_out, 16)
        return carry

    lax.fori_loop(0, 12, edges, 0)

    def channel_norm(g, carry):
        span = pl.ds(pl.multiple_of(g * 32, 32), 32)
        total = jnp.zeros((32, 128), F32)
        square = jnp.zeros((32, 128), F32)
        for k in range(12):
            part = conv[k, span, :]
            total = total + part
            square = square + part * part
        mean = jnp.sum(total, axis=1, keepdims=True) / 1536
        var = jnp.sum(square, axis=1, keepdims=True) / 1536 - mean * mean
        scale = lax.rsqrt(var + 1e-05)
        for k in range(12):
            part = (conv[k, span, :] - mean) * scale * taps[k, 31:32, :]
            mixed[span, k * 128:(k + 1) * 128] = (part * jax.nn.sigmoid(part)).astype(BF)
        return carry

    lax.fori_loop(0, 4, channel_norm, 0)

    slot = lax.broadcasted_iota(jnp.int32, (CAP * N, N), 0)
    i, r = slot // CAP, slot % CAP
    dz, dy, dx, dc = offsets(i)
    z, y, x = (sp // 16 + dz) % 4, ((sp // 4) % 4 + dy) % 4, (sp % 4 + dx) % 4
    expert = ((z * 4 + y) * 4 + x) * 2 + (tp + dc) % 2
    first = ids_ref[0:1, :] == expert
    second = ids_ref[1:2, :] == expert
    named = jnp.where(first | second, 1.0, 0.0)
    rows = lax.broadcasted_iota(jnp.int32, (N, N), 0)
    cols = lax.broadcasted_iota(jnp.int32, (N, N), 1)
    before = jnp.where(rows < cols, 1.0, 0.0).astype(BF)
    rank = jnp.dot(named.astype(BF), before, preferred_element_type=F32)
    chosen = jnp.where(rank == r.astype(F32), named, 0.0)
    gates[...] = chosen.astype(BF)
    weight = jnp.transpose(chosen * jnp.where(first, mix_ref[0:1, :], mix_ref[1:2, :]))
    high = weight.astype(BF)
    wt_hi[...] = high
    wt_lo[...] = (weight - high.astype(F32)).astype(BF)

    resid_copy.wait()
    ow_copy.wait()

    def project(j, squares):
        col = pl.ds(pl.multiple_of(j * TILE, TILE), TILE)
        part = jnp.dot(mixed[...], ow[:, col], preferred_element_type=F32)
        total = (resid[:, col].astype(F32) + part).astype(BF)
        stream[:, col] = total
        wide = total.astype(F32)
        return squares + jnp.sum(wide * wide, axis=1, keepdims=True)

    squares = lax.fori_loop(0, 4, project, jnp.zeros((N, 1), F32))
    scale = lax.rsqrt(squares / 2048 + 1e-06)

    def fill(k, carry):
        col = pl.ds(pl.multiple_of(k * TILE, TILE), TILE)
        normed = (stream[:, col].astype(F32) * scale * ffn_gain_ref[:, col]).astype(BF)
        for g in range(4):
            part = jnp.dot(
                gates[g * 128:(g + 1) * 128, :], normed, preferred_element_type=F32
            ).astype(BF)
            sendbuf[g * 32:(g + 1) * 32, :, col] = part.reshape(32, CAP, TILE)
        return carry

    lax.fori_loop(0, 4, fill, 0)
    recvbuf[0] = sendbuf[0]
    pl.semaphore_wait(z_ready, 3)

    def dispatch(chunk):
        def one(i, carry):
            pltpu.make_async_remote_copy(
                src_ref=sendbuf.at[i], dst_ref=recvbuf.at[i],
                send_sem=dsend, recv_sem=drecv.at[chunk],
                device_id=device_at(i, 1), device_id_type=MESH,
            ).start()
            return carry

        lax.fori_loop(max(1, chunk * HALF), (chunk + 1) * HALF, one, 0)

    def giveback(chunk):
        def one(i, carry):
            pltpu.make_async_remote_copy(
                src_ref=ysend.at[i], dst_ref=yrecv.at[i],
                send_sem=rsend, recv_sem=rrecv.at[chunk],
                device_id=device_at(i, -1), device_id_type=MESH,
            ).start()
            return carry

        lax.fori_loop(max(1, chunk * HALF), (chunk + 1) * HALF, one, 0)

    def whole(chunk, source, target, send, recv):
        low = max(1, chunk * HALF)
        span = pl.ds(low, (chunk + 1) * HALF - low)
        return pltpu.make_async_remote_copy(
            src_ref=source.at[span], dst_ref=target.at[span], send_sem=send,
            recv_sem=recv.at[chunk], device_id=device_at(1, 1), device_id_type=MESH,
        )

    dispatch(0)
    dispatch(1)
    rows_chunk = HALF * CAP
    for chunk in range(2):
        whole(chunk, sendbuf, recvbuf, dsend, drecv).wait_recv()
        if chunk == 0:
            for copy in weights:
                copy.wait()

        def gather(g, carry):
            span = pl.ds(pl.multiple_of(g * 64, 64), 64)
            xs[span, :] = recvbuf[pl.ds(chunk * HALF + g * 16, 16)].reshape(64, 2048)
            return carry

        lax.fori_loop(0, 4, gather, 0)

        def up(j, carry):
            col = pl.ds(pl.multiple_of(j * TILE, TILE), TILE)
            gate = jnp.dot(xs[...], wg[:, col], preferred_element_type=F32)
            value = jnp.dot(xs[...], wu[:, col], preferred_element_type=F32)
            hid[:, col] = (gate * jax.nn.sigmoid(gate) * value).astype(BF)
            return carry

        lax.fori_loop(0, 1024 // TILE, up, 0)

        def down(j, carry):
            col = pl.ds(pl.multiple_of(j * TILE, TILE), TILE)
            part = jnp.dot(hid[...], wd[:, col], preferred_element_type=F32).astype(BF)
            ysend[chunk * HALF:(chunk + 1) * HALF, :, col] = part.reshape(HALF, CAP, TILE)
            return carry

        lax.fori_loop(0, 2048 // TILE, down, 0)
        if chunk == 0:
            yrecv[0] = ysend[0]
        giveback(chunk)

    for chunk in range(2):
        whole(chunk, ysend, yrecv, rsend, rrecv).wait_recv()
        slots = slice(chunk * rows_chunk, (chunk + 1) * rows_chunk)
        lhs_hi, lhs_lo = wt_hi[:, slots], wt_lo[:, slots]

        def combine(j, carry):
            col = pl.ds(pl.multiple_of(j * TILE, TILE), TILE)
            got = yrecv[chunk * HALF:(chunk + 1) * HALF, :, col].reshape(rows_chunk, TILE)
            part = jnp.dot(lhs_hi, got, preferred_element_type=F32)
            part = part + jnp.dot(lhs_lo, got, preferred_element_type=F32)
            if chunk == 0:
                acc[:, col] = part + stream[:, col].astype(F32)
            else:
                out_ref[:, col] = acc[:, col] + part
            return carry

        lax.fori_loop(0, 2048 // TILE, combine, 0)
    for chunk in range(2):
        whole(chunk, sendbuf, recvbuf, dsend, drecv).wait_send()
        whole(chunk, ysend, yrecv, rsend, rrecv).wait_send()
    to_peer.wait_send()
    taps_to_peer.wait_send()
    gain_to_peer.wait_send()

    @pl.when(sp < 63)
    def _():
        to_next.wait_send()

    @pl.when(sp > 0)
    def _():
        to_previous.wait_send()


def per_device(
    resid,
    value_in,
    gate_in,
    conv_weight,
    norm_gain,
    out_weight,
    ffn_gain,
    expert_ids,
    expert_mix,
    w_gate,
    w_up,
    w_down,
):
    vmem = pl.BlockSpec(memory_space=pltpu.VMEM)
    hbm = pl.BlockSpec(memory_space=pltpu.HBM)
    slots = pltpu.VMEM((N, CAP, 2048), BF)
    dma = pltpu.SemaphoreType.DMA
    total = pl.pallas_call(
        layer_kernel,
        out_shape=jax.ShapeDtypeStruct((N, 2048), F32),
        in_specs=[hbm, vmem, vmem, vmem, vmem, hbm, vmem, vmem, vmem, hbm, hbm, hbm],
        out_specs=vmem,
        scratch_shapes=[
            pltpu.VMEM((2048, 1024), BF),
            pltpu.VMEM((2048, 1024), BF),
            pltpu.VMEM((1024, 2048), BF),
            pltpu.VMEM((1536, 2048), BF),
            pltpu.VMEM((N, 2048), BF),
            pltpu.VMEM((12, 32, 128), F32),
            pltpu.VMEM((31, 768), F32),
            pltpu.VMEM((768,), F32),
            pltpu.VMEM((256, 768), BF),
            pltpu.VMEM((144, 768), BF),
            pltpu.VMEM((2, 16, 768), BF),
            pltpu.VMEM((12, 160, 128), F32),
            pltpu.VMEM((12, 128, 128), F32),
            pltpu.VMEM((N, 1536), BF),
            pltpu.VMEM((N, 2048), BF),
            pltpu.VMEM((N, 2048), BF),
            slots, slots, slots, slots,
            pltpu.VMEM((HALF * CAP, 2048), BF),
            pltpu.VMEM((HALF * CAP, 1024), BF),
            pltpu.VMEM((CAP * N, N), BF),
            pltpu.VMEM((N, CAP * N), BF),
            pltpu.VMEM((N, CAP * N), BF),
            pltpu.VMEM((N, 2048), F32),
            dma((5,)), dma((2,)), dma((2,)), dma, dma, dma((2,)), dma((2,)), dma, dma((2,)), dma, dma((2,)),
            pltpu.SemaphoreType.REGULAR, pltpu.SemaphoreType.REGULAR,
        ],
        compiler_params=pltpu.CompilerParams(
            collective_id=0, has_side_effects=True, vmem_limit_bytes=60 * 2**20
        ),
        name="layer",
    )(
        resid, value_in, gate_in, conv_weight, norm_gain, out_weight,
        ffn_gain.reshape(1, 2048), expert_ids.T, expert_mix.T, w_gate[0], w_up[0], w_down[0],
    )
    return total.astype(BF)


def solution(mesh):
    return jax.shard_map(
        per_device,
        mesh=mesh,
        in_specs=(
            P(("sp", "tp"), None),
            P("sp", "tp"),
            P("sp", "tp"),
            P(None, "tp"),
            P("tp"),
            P(),
            P(),
            P(("sp", "tp"), None),
            P(("sp", "tp"), None),
            P(("sp", "tp"), None, None),
            P(("sp", "tp"), None, None),
            P(("sp", "tp"), None, None),
        ),
        out_specs=P(("sp", "tp"), None),
        check_vma=False,
    )
```

time: 101 us -> 71.9 us (0.71)
  local copies, waits for them, and re-layouts: 7.55 us -> 0 us
  blocking collectives: 7.1 us -> 0 us
  starting transfers between devices: 5.23 us -> 0 us
  other arithmetic: 6.92 us -> 2.09 us
  matrix products: 3.9 us -> 0 us
    ppermute x2 -> x0, starting transfers between devices: 5.23 us -> none  [the longest x1 3.93 us: padded_2(): lax.ppermute(lax.slice_in_dim(block, block.shape[dim] - width, None, axis...]
    unnamed x11 -> x0, local copies, waits for them, and re-layouts: 4.71 us -> none
    reduce_sum x1 -> x0, other arithmetic: 4.16 us -> none  [per_device(): sums = lax.psum((jnp.sum(conv, axis=1), jnp.sum(conv * conv, axis=1)), 'tp')]
    all_to_all x1 -> x0, blocking collectives: 4.02 us -> none  [per_device(): lax.all_to_all(mixed, 'tp', split_axis=0, concat_axis=1, tiled=True)]
    dot_general x1 -> x0, matrix products: 3.9 us -> none  [per_device(): proj = jnp.dot(regrouped, out_weight, preferred_element_type=F32)]
    psum x1 -> x0, blocking collectives: 3.08 us -> none  [per_device(): sums = lax.psum((jnp.sum(conv, axis=1), jnp.sum(conv * conv, axis=1)), 'tp')]
    slice x3 -> x0, local copies, waits for them, and re-layouts: 2.63 us -> none  [the longest x2 2.62 us: per_device(): conv = conv + padded[tap:tap + length] * conv_weight[tap]]
    convert_element_type x4 -> x1, other arithmetic: 2.74 us -> 2.09 us  [per_device(): return total.astype(BF)]
  transfers between devices with their start and end apart: 2 -> 0, of which waited for: 0 -> 0; matrix products, arithmetic and copies ran while one was open for 5% -> 0% of each run, Pallas kernels for 0% -> 0%
where the time goes in v2:
time: 71.9 us; the launch traced here: 71.8 us
  Pallas kernels  69.7 us (97%)
  other arithmetic  2.09 us (3%)
    pallas_call x1, Pallas kernels, per_device(): pl.pallas_call(layer_kernel, out_shape=jax.ShapeDtypeStruct((N, 2048), F3...  69.7 us
    convert_element_type x1, other arithmetic, per_device(): return total.astype(BF)  2.09 us

profile of v2, /device:TPU:1, one launch (start us, length us, event | category | flops | bytes accessed | tf_op | source)
XLA Modules:
  0.0 71.8 jit_solution(4595113875973598769)
XLA Ops:
  0.0 69.7 %layer.1 = f32[128,2048]{1,0:T(8,128)} custom-call(bf16[128,2048]{1,0:T(8,128)(2,1)} %resid_hbm.1, bf16[256,768]{1,0:T(8,128)(2,1)} %value_ref.1, bf16[256,768]{1,0:T(8,128)(2,1)} %gate_ref.1, f32[31,768]{1,0:T(8,128)} %taps_in.1, f32[768]{0:T(1024)} %gain_in.1, bf16[1536,2048]{1,0:T(8,128)(2,1)} %ow_hbm.1, f32[1,2048]{1,0:T(1,128)} %bitcast.9, ...), custom_call_target="tpu_custom_call" | custom-call | tf_op jit(solution)/shard_map/layer/pallas_call | solution.py:365
  69.7 2.1 %convert_element_type.3 = bf16[128,2048]{1,0:T(8,128)(2,1)} convert(f32[128,2048]{1,0:T(8,128)} %layer.1) | non-fusion elementwise | flops 262144 | bytes 1572864 | tf_op jit(solution)/shard_map/convert_element_type | solution.py:405

commit v3 on v2

v3 whole, which is shorter than its diff:
```python
import functools

import jax
import jax.numpy as jnp
from jax import lax
from jax.experimental import pallas as pl
from jax.experimental.pallas import tpu as pltpu
from jax.sharding import PartitionSpec as P

MESH = pl.DeviceIdType.MESH
BF = jnp.bfloat16
F32 = jnp.float32
CAP = 4
N = 128
TILE = 512
CHUNKS = 4
PEERS = N // CHUNKS
ROWS = PEERS * CAP


def offsets(i):
    a, b, c = i % 4, (i // 4) % 4, (i // 16) % 4
    return a, (a + b) % 4, (a + b + c) % 4, i // 64


def device_at(i, sign):
    sp, tp = lax.axis_index("sp"), lax.axis_index("tp")
    dz, dy, dx, dc = offsets(i)
    z, y, x = sp // 16, (sp // 4) % 4, sp % 4
    z, y, x = (z + 4 + sign * dz) % 4, (y + 4 + sign * dy) % 4, (x + 4 + sign * dx) % 4
    return (z * 4 + y) * 4 + x, (tp + dc) % 2


def device_in_line(dz, dy, dx, dc):
    sp, tp = lax.axis_index("sp"), lax.axis_index("tp")
    z, y, x = (sp // 16 + dz) % 4, ((sp // 4) % 4 + dy) % 4, (sp % 4 + dx) % 4
    return (z * 4 + y) * 4 + x, (tp + dc) % 2


def layer_kernel(
    resid_hbm, value_hbm, gate_hbm, taps_hbm, gain_hbm, ow_hbm, ffn_gain_hbm, ids_hbm, mix_hbm,
    wg_hbm, wu_hbm, wd_hbm,
    out_ref,
    value, gate, taps_in, gain_in, ffn_gain, ids, mix, resid, ow, wg, wu, wd,
    taps, taps_other, gain_other, glu, other, halo, padded, conv, mixed, stream, normed,
    sendbuf, recvbuf, ysend, yrecv, xs, hid, gates, wt, acc,
    insem, gsend, grecv, hsend, hrecv, dsend, drecv, rsend, rrecv, y_ready, z_ready,
):
    sp, tp = lax.axis_index("sp"), lax.axis_index("tp")
    barrier = pltpu.get_barrier_semaphore()

    def signal(semaphore, device):
        pl.semaphore_signal(semaphore, inc=1, device_id=device, device_id_type=MESH)

    halo_from = jnp.where(tp == 0, sp - 1, sp + 1)
    has_halo = (halo_from >= 0) & (halo_from < 64)

    @pl.when(has_halo)
    def _():
        signal(barrier, (halo_from, 0))
        signal(barrier, (halo_from, 1))

    for step in (2, 3, 1):
        signal(barrier, device_in_line(0, step, 0, 0))
        signal(barrier, device_in_line(step, 0, 0, 0))
    for dc in range(2):
        for dx in range(4):
            if dx or dc:
                signal(barrier, device_in_line(0, 0, dx, dc))

    fetched = [
        pltpu.make_async_copy(source, target, insem.at[n])
        for n, (source, target) in enumerate([
            (value_hbm, value), (gate_hbm, gate), (taps_hbm, taps_in), (gain_hbm, gain_in),
            (ids_hbm, ids), (mix_hbm, mix), (ffn_gain_hbm, ffn_gain), (resid_hbm, resid),
            (ow_hbm, ow), (wg_hbm, wg), (wu_hbm, wu), (wd_hbm, wd),
        ])
    ]
    for copy in fetched:
        copy.start()
    for copy in fetched[:4]:
        copy.wait()

    def gated(g, carry):
        span = pl.ds(pl.multiple_of(g * 32, 32), 32)
        wide = value[span, :].astype(F32)
        glu[span, :] = (wide * jax.nn.sigmoid(gate[span, :].astype(F32))).astype(BF)
        return carry

    lax.fori_loop(0, 8, gated, 0)

    own_rows = pl.multiple_of(112 * tp, 16)
    inner = pl.multiple_of(16 * (1 - tp), 16)
    edge = pl.multiple_of(144 * tp, 16)
    inner_out = inner
    edge_out = pl.multiple_of(112 * tp, 16)

    def place(first, rows_of, taps_of, gain_of):
        for k in range(6):
            lanes = slice(k * 128, (k + 1) * 128)
            padded[first + k, pl.ds(inner, 144), :] = rows_of(lanes).astype(F32)
            taps[first + k, 0:31, :] = taps_of[:, lanes]
            taps[first + k, 31:32, :] = gain_of[lanes].reshape(1, 128)

    def convolve(block, start, count):
        total = jnp.zeros((count, 128), F32)
        for tap in range(31):
            total = total + padded[block, pl.ds(start + tap + 1, count), :] * taps[
                block, tap:tap + 1, :
            ]
        conv[block, pl.ds(start, count), :] = total

    def inner_blocks(first):
        def one(k, carry):
            convolve(first + k, inner_out, 56)
            convolve(first + k, inner_out + 56, 56)
            return carry

        lax.fori_loop(0, 6, one, 0)

    place(tp * 6, lambda lanes: glu[pl.ds(own_rows, 144), lanes], taps_in, gain_in)
    inner_blocks(tp * 6)
    expected = 13 + jnp.where(sp > 0, 1, 0) + jnp.where(sp < 63, 1, 0)
    pl.semaphore_wait(barrier, expected)

    to_next = pltpu.make_async_remote_copy(
        src_ref=glu.at[pl.ds(240, 16)], dst_ref=halo.at[tp], send_sem=hsend.at[0],
        recv_sem=hrecv.at[tp], device_id=(sp + 1, 0), device_id_type=MESH,
    )
    to_previous = pltpu.make_async_remote_copy(
        src_ref=glu.at[pl.ds(0, 16)], dst_ref=halo.at[tp], send_sem=hsend.at[1],
        recv_sem=hrecv.at[tp], device_id=(sp - 1, 1), device_id_type=MESH,
    )

    @pl.when(sp < 63)
    def _():
        to_next.start()

    @pl.when(sp > 0)
    def _():
        to_previous.start()

    for step in (2, 3, 1):
        signal(y_ready, device_in_line(0, step, 0, 0))
    peer_rows = pl.ds(pl.multiple_of(112 * (1 - tp), 16), 144)
    to_peer = [
        pltpu.make_async_remote_copy(
            src_ref=source, dst_ref=target, send_sem=gsend.at[n], recv_sem=grecv.at[n],
            device_id=(sp, 1 - tp), device_id_type=MESH,
        )
        for n, (source, target) in enumerate(
            [(glu.at[peer_rows], other), (taps_in, taps_other), (gain_in, gain_other)]
        )
    ]
    for copy in to_peer:
        copy.start()
    for copy in fetched[4:6]:
        copy.wait()

    slot = lax.broadcasted_iota(jnp.int32, (CAP * N, N), 0)
    i, r = slot // CAP, slot % CAP
    dz, dy, dx, dc = offsets(i)
    z, y, x = (sp // 16 + dz) % 4, ((sp // 4) % 4 + dy) % 4, (sp % 4 + dx) % 4
    expert = ((z * 4 + y) * 4 + x) * 2 + (tp + dc) % 2
    first = ids[0:1, :] == expert
    second = ids[1:2, :] == expert
    named = jnp.where(first | second, 1.0, 0.0)
    rows = lax.broadcasted_iota(jnp.int32, (N, N), 0)
    cols = lax.broadcasted_iota(jnp.int32, (N, N), 1)
    before = jnp.where(rows < cols, 1.0, 0.0).astype(BF)
    rank = jnp.dot(named.astype(BF), before, preferred_element_type=F32)
    chosen = jnp.where(rank == r.astype(F32), named, 0.0)
    gates[...] = chosen.astype(BF)
    weight = jnp.transpose(chosen * jnp.where(first, mix[0:1, :], mix[1:2, :]))
    high = weight.astype(BF)
    wt[0:N, :] = high
    wt[N:2 * N, :] = (weight - high.astype(F32)).astype(BF)

    for copy in to_peer:
        copy.wait_recv()
    place((1 - tp) * 6, lambda lanes: other[:, lanes], taps_other, gain_other)
    inner_blocks((1 - tp) * 6)
    pl.semaphore_wait(y_ready, 3)
    for step in (2, 3, 1):
        signal(z_ready, device_in_line(step, 0, 0, 0))

    def channel_norm(start, count):
        span = pl.ds(start, count)
        total = jnp.zeros((count, 128), F32)
        square = jnp.zeros((count, 128), F32)
        for k in range(12):
            part = conv[k, span, :]
            total = total + part
            square = square + part * part
        mean = jnp.sum(total, axis=1, keepdims=True) / 1536
        var = jnp.sum(square, axis=1, keepdims=True) / 1536 - mean * mean
        scale = lax.rsqrt(var + 1e-05)
        for k in range(12):
            part = (conv[k, span, :] - mean) * scale * taps[k, 31:32, :]
            mixed[span, k * 128:(k + 1) * 128] = (part * jax.nn.sigmoid(part)).astype(BF)

    def inner_norm(g, carry):
        channel_norm(pl.multiple_of(inner_out + g * 16, 16), 16)
        return carry

    lax.fori_loop(0, 7, inner_norm, 0)

    @pl.when(has_halo)
    def _():
        for c in range(2):
            pltpu.make_async_remote_copy(
                src_ref=glu.at[pl.ds(0, 16)], dst_ref=halo.at[c], send_sem=hsend.at[0],
                recv_sem=hrecv.at[c], device_id=(sp, 1 - tp), device_id_type=MESH,
            ).wait_recv()
            for k in range(6):
                lanes = slice(k * 128, (k + 1) * 128)
                padded[c * 6 + k, pl.ds(edge, 16), :] = halo[c, :, lanes].astype(F32)

    @pl.when(jnp.logical_not(has_halo))
    def _():
        for k in range(12):
            padded[k, pl.ds(edge, 16), :] = jnp.zeros((16, 128), F32)

    def edges(k, carry):
        convolve(k, edge_out, 16)
        return carry

    lax.fori_loop(0, 12, edges, 0)
    channel_norm(edge_out, 16)
    for copy in fetched[6:9]:
        copy.wait()

    def project(j, squares):
        col = pl.ds(pl.multiple_of(j * TILE, TILE), TILE)
        part = jnp.dot(mixed[...], ow[:, col], preferred_element_type=F32)
        total = (resid[:, col].astype(F32) + part).astype(BF)
        stream[:, col] = total
        wide = total.astype(F32)
        return squares + jnp.sum(wide * wide, axis=1, keepdims=True)

    squares = lax.fori_loop(0, 4, project, jnp.zeros((N, 1), F32))
    scale = lax.rsqrt(squares / 2048 + 1e-06)
    for k in range(4):
        col = slice(k * TILE, (k + 1) * TILE)
        normed[:, col] = (stream[:, col].astype(F32) * scale * ffn_gain[:, col]).astype(BF)
    pl.semaphore_wait(z_ready, 3)

    def send_all(chunk, source, target, send, recv, sign):
        def one(i, carry):
            pltpu.make_async_remote_copy(
                src_ref=source.at[i], dst_ref=target.at[i], send_sem=send,
                recv_sem=recv.at[chunk], device_id=device_at(i, sign), device_id_type=MESH,
            ).start()
            return carry

        lax.fori_loop(max(1, chunk * PEERS), (chunk + 1) * PEERS, one, 0)

    def whole(chunk, source, target, send, recv):
        low = max(1, chunk * PEERS)
        span = pl.ds(low, (chunk + 1) * PEERS - low)
        return pltpu.make_async_remote_copy(
            src_ref=source.at[span], dst_ref=target.at[span], send_sem=send,
            recv_sem=recv.at[chunk], device_id=device_at(1, 1), device_id_type=MESH,
        )

    for chunk in range(CHUNKS):
        def fill(k, carry):
            col = pl.ds(pl.multiple_of(k * TILE, TILE), TILE)
            part = jnp.dot(
                gates[chunk * ROWS:(chunk + 1) * ROWS, :], normed[:, col],
                preferred_element_type=F32,
            ).astype(BF)
            sendbuf[chunk * PEERS:(chunk + 1) * PEERS, :, col] = part.reshape(PEERS, CAP, TILE)
            return carry

        lax.fori_loop(0, 4, fill, 0)
        send_all(chunk, sendbuf, recvbuf, dsend, drecv, 1)
    recvbuf[0] = sendbuf[0]
    for copy in fetched[9:]:
        copy.wait()

    for chunk in range(CHUNKS):
        whole(chunk, sendbuf, recvbuf, dsend, drecv).wait_recv()
        peers = slice(chunk * PEERS, (chunk + 1) * PEERS)
        xs[...] = recvbuf[peers].reshape(ROWS, 2048)

        def up(j, carry):
            col = pl.ds(pl.multiple_of(j * TILE, TILE), TILE)
            gated_part = jnp.dot(xs[...], wg[:, col], preferred_element_type=F32)
            up_part = jnp.dot(xs[...], wu[:, col], preferred_element_type=F32)
            hid[:, col] = (gated_part * jax.nn.sigmoid(gated_part) * up_part).astype(BF)
            return carry

        lax.fori_loop(0, 1024 // TILE, up, 0)

        def down(j, carry):
            col = pl.ds(pl.multiple_of(j * TILE, TILE), TILE)
            part = jnp.dot(hid[...], wd[:, col], preferred_element_type=F32).astype(BF)
            ysend[peers, :, col] = part.reshape(PEERS, CAP, TILE)
            return carry

        lax.fori_loop(0, 2048 // TILE, down, 0)
        if chunk == 0:
            yrecv[0] = ysend[0]
        send_all(chunk, ysend, yrecv, rsend, rrecv, -1)

    for chunk in range(CHUNKS):
        whole(chunk, ysend, yrecv, rsend, rrecv).wait_recv()
        peers = slice(chunk * PEERS, (chunk + 1) * PEERS)

        def combine(j, carry):
            col = pl.ds(pl.multiple_of(j * TILE, TILE), TILE)
            got = yrecv[peers, :, col].reshape(ROWS, TILE)
            both = jnp.dot(
                wt[:, chunk * ROWS:(chunk + 1) * ROWS], got, preferred_element_type=F32
            )
            part = both[0:N] + both[N:2 * N]
            if chunk == 0:
                acc[:, col] = part + stream[:, col].astype(F32)
            elif chunk < CHUNKS - 1:
                acc[:, col] = acc[:, col] + part
            else:
                out_ref[:, col] = acc[:, col] + part
            return carry

        lax.fori_loop(0, 2048 // TILE, combine, 0)

    for chunk in range(CHUNKS):
        whole(chunk, sendbuf, recvbuf, dsend, drecv).wait_send()
        whole(chunk, ysend, yrecv, rsend, rrecv).wait_send()
    for copy in to_peer:
        copy.wait_send()

    @pl.when(sp < 63)
    def _():
        to_next.wait_send()

    @pl.when(sp > 0)
    def _():
        to_previous.wait_send()


def per_device(
    resid,
    value_in,
    gate_in,
    conv_weight,
    norm_gain,
    out_weight,
    ffn_gain,
    expert_ids,
    expert_mix,
    w_gate,
    w_up,
    w_down,
):
    vmem = pl.BlockSpec(memory_space=pltpu.VMEM)
    hbm = pl.BlockSpec(memory_space=pltpu.HBM)
    slots = pltpu.VMEM((N, CAP, 2048), BF)
    dma = pltpu.SemaphoreType.DMA
    total = pl.pallas_call(
        layer_kernel,
        out_shape=pltpu.VMEM((N, 2048), F32),
        in_specs=[hbm] * 12,
        out_specs=vmem,
        scratch_shapes=[
            pltpu.VMEM((256, 768), BF),
            pltpu.VMEM((256, 768), BF),
            pltpu.VMEM((31, 768), F32),
            pltpu.VMEM((768,), F32),
            pltpu.VMEM((1, 2048), F32),
            pltpu.VMEM((2, N), jnp.int32),
            pltpu.VMEM((2, N), F32),
            pltpu.VMEM((N, 2048), BF),
            pltpu.VMEM((1536, 2048), BF),
            pltpu.VMEM((2048, 1024), BF),
            pltpu.VMEM((2048, 1024), BF),
            pltpu.VMEM((1024, 2048), BF),
            pltpu.VMEM((12, 32, 128), F32),
            pltpu.VMEM((31, 768), F32),
            pltpu.VMEM((768,), F32),
            pltpu.VMEM((256, 768), BF),
            pltpu.VMEM((144, 768), BF),
            pltpu.VMEM((2, 16, 768), BF),
            pltpu.VMEM((12, 160, 128), F32),
            pltpu.VMEM((12, 128, 128), F32),
            pltpu.VMEM((N, 1536), BF),
            pltpu.VMEM((N, 2048), BF),
            pltpu.VMEM((N, 2048), BF),
            slots, slots, slots, slots,
            pltpu.VMEM((ROWS, 2048), BF),
            pltpu.VMEM((ROWS, 1024), BF),
            pltpu.VMEM((CAP * N, N), BF),
            pltpu.VMEM((2 * N, CAP * N), BF),
            pltpu.VMEM((N, 2048), F32),
            dma((12,)), dma((3,)), dma((3,)), dma((2,)), dma((2,)), dma, dma((CHUNKS,)), dma,
            dma((CHUNKS,)), pltpu.SemaphoreType.REGULAR, pltpu.SemaphoreType.REGULAR,
        ],
        compiler_params=pltpu.CompilerParams(
            collective_id=0, has_side_effects=True, vmem_limit_bytes=60 * 2**20
        ),
        name="layer",
    )(
        resid, value_in, gate_in, conv_weight, norm_gain, out_weight,
        ffn_gain.reshape(1, 2048), expert_ids.T, expert_mix.T, w_gate[0], w_up[0], w_down[0],
    )
    return total.astype(BF)


def solution(mesh):
    return jax.shard_map(
        per_device,
        mesh=mesh,
        in_specs=(
            P(("sp", "tp"), None),
            P("sp", "tp"),
            P("sp", "tp"),
            P(None, "tp"),
            P("tp"),
            P(),
            P(),
            P(("sp", "tp"), None),
            P(("sp", "tp"), None),
            P(("sp", "tp"), None, None),
            P(("sp", "tp"), None, None),
            P(("sp", "tp"), None, None),
        ),
        out_specs=P(("sp", "tp"), None),
        check_vma=False,
    )
```

time: 71.9 us -> 67.1 us (0.933)
  Pallas kernels: 69.7 us -> 66.1 us
  other arithmetic: 2.09 us -> 0.86 us
    pallas_call x1, Pallas kernels: 69.7 us -> 66.1 us  [per_device(): pl.pallas_call(layer_kernel, out_shape=pltpu.VMEM((N, 2048), F32), in_spe...]
    convert_element_type x1, other arithmetic: 2.09 us -> 0.86 us  [per_device(): return total.astype(BF)]
where the time goes in v3:
time: 67.1 us; the launch traced here: 67 us
  Pallas kernels  66.1 us (99%)
  other arithmetic  0.86 us (1%)
    pallas_call x1, Pallas kernels, per_device(): pl.pallas_call(layer_kernel, out_shape=pltpu.VMEM((N, 2048), F32), in_spe...  66.1 us

profile of v3, /device:TPU:1, one launch (start us, length us, event | category | flops | bytes accessed | tf_op | source)
XLA Modules:
  0.0 67.0 jit_solution(6516107856460949532)
XLA Ops:
  0.0 66.1 %layer.1 = f32[128,2048]{1,0:T(8,128)S(1)} custom-call(bf16[128,2048]{1,0:T(8,128)(2,1)} %resid_hbm.1, bf16[256,768]{1,0:T(8,128)(2,1)} %value_hbm.1, bf16[256,768]{1,0:T(8,128)(2,1)} %gate_hbm.1, f32[31,768]{1,0:T(8,128)} %taps_hbm.1, f32[768]{0:T(1024)} %gain_hbm.1, bf16[1536,2048]{1,0:T(8,128)(2,1)} %ow_hbm.1, f32[1,2048]{1,0:T(1,128)} %bitcast.9, ...), custom_call_target="tpu_custom_call" | custom-call | tf_op jit(solution)/shard_map/layer/pallas_call | solution.py:361
  66.1 0.9 %convert_element_type.3 = bf16[128,2048]{1,0:T(8,128)(2,1)} convert(f32[128,2048]{1,0:T(8,128)S(1)} %layer.1) | non-fusion elementwise | flops 262144 | bytes 1572864 | tf_op jit(solution)/shard_map/convert_element_type | solution.py:407

commit v4 on v3

--- a/solution.py
+++ b/solution.py
@@ -14,13 +14,19 @@
 N = 128
 TILE = 512
 CHUNKS = 4
+BACK = 4
 PEERS = N // CHUNKS
 ROWS = PEERS * CAP
+GATHER = 256
 
 
 def offsets(i):
     a, b, c = i % 4, (i // 4) % 4, (i // 16) % 4
     return a, (a + b) % 4, (a + b + c) % 4, i // 64
+
+
+def sigmoid(v):
+    return 0.5 * jnp.tanh(0.5 * v) + 0.5
 
 
 def device_at(i, sign):
@@ -42,7 +48,7 @@
     wg_hbm, wu_hbm, wd_hbm,
     out_ref,
     value, gate, taps_in, gain_in, ffn_gain, ids, mix, resid, ow, wg, wu, wd,
-    taps, taps_other, gain_other, glu, other, halo, padded, conv, mixed, stream, normed,
+    taps, taps_other, gain_other, glu, other, halo, padded, conv, mixed, stream,
     sendbuf, recvbuf, ysend, yrecv, xs, hid, gates, wt, acc,
     insem, gsend, grecv, hsend, hrecv, dsend, drecv, rsend, rrecv, y_ready, z_ready,
 ):
@@ -84,7 +90,7 @@
     def gated(g, carry):
         span = pl.ds(pl.multiple_of(g * 32, 32), 32)
         wide = value[span, :].astype(F32)
-        glu[span, :] = (wide * jax.nn.sigmoid(gate[span, :].astype(F32))).astype(BF)
+        glu[span, :] = (wide * sigmoid(gate[span, :].astype(F32))).astype(BF)
         return carry
 
     lax.fori_loop(0, 8, gated, 0)
@@ -197,13 +203,9 @@
         scale = lax.rsqrt(var + 1e-05)
         for k in range(12):
             part = (conv[k, span, :] - mean) * scale * taps[k, 31:32, :]
-            mixed[span, k * 128:(k + 1) * 128] = (part * jax.nn.sigmoid(part)).astype(BF)
-
-    def inner_norm(g, carry):
-        channel_norm(pl.multiple_of(inner_out + g * 16, 16), 16)
-        return carry
-
-    lax.fori_loop(0, 7, inner_norm, 0)
+            mixed[span, k * 128:(k + 1) * 128] = (part * sigmoid(part)).astype(BF)
+
+    channel_norm(inner_out, 112)
 
     @pl.when(has_halo)
     def _():
@@ -222,30 +224,29 @@
             padded[k, pl.ds(edge, 16), :] = jnp.zeros((16, 128), F32)
 
     def edges(k, carry):
-        convolve(k, edge_out, 16)
+        for part in range(4):
+            convolve(4 * k + part, edge_out, 16)
         return carry
 
-    lax.fori_loop(0, 12, edges, 0)
+    lax.fori_loop(0, 3, edges, 0)
     channel_norm(edge_out, 16)
     for copy in fetched[6:9]:
         copy.wait()
 
-    def project(j, squares):
-        col = pl.ds(pl.multiple_of(j * TILE, TILE), TILE)
+    for j in range(2048 // TILE):
+        col = slice(j * TILE, (j + 1) * TILE)
         part = jnp.dot(mixed[...], ow[:, col], preferred_element_type=F32)
         total = (resid[:, col].astype(F32) + part).astype(BF)
         stream[:, col] = total
-        wide = total.astype(F32)
-        return squares + jnp.sum(wide * wide, axis=1, keepdims=True)
-
-    squares = lax.fori_loop(0, 4, project, jnp.zeros((N, 1), F32))
-    scale = lax.rsqrt(squares / 2048 + 1e-06)
-    for k in range(4):
-        col = slice(k * TILE, (k + 1) * TILE)
-        normed[:, col] = (stream[:, col].astype(F32) * scale * ffn_gain[:, col]).astype(BF)
+        for group in range(512 // GATHER):
+            part = jnp.dot(
+                gates[group * GATHER:(group + 1) * GATHER, :], total, preferred_element_type=F32
+            ).astype(BF)
+            peers = slice(group * GATHER // CAP, (group + 1) * GATHER // CAP)
+            sendbuf[peers, :, col] = part.reshape(GATHER // CAP, CAP, TILE)
     pl.semaphore_wait(z_ready, 3)
 
-    def send_all(chunk, source, target, send, recv, sign):
+    def send_all(chunk, source, target, send, recv, sign, peers=PEERS):
         def one(i, carry):
             pltpu.make_async_remote_copy(
                 src_ref=source.at[i], dst_ref=target.at[i], send_sem=send,
@@ -253,27 +254,17 @@
             ).start()
             return carry
 
-        lax.fori_loop(max(1, chunk * PEERS), (chunk + 1) * PEERS, one, 0)
-
-    def whole(chunk, source, target, send, recv):
-        low = max(1, chunk * PEERS)
-        span = pl.ds(low, (chunk + 1) * PEERS - low)
+        lax.fori_loop(max(1, chunk * peers), (chunk + 1) * peers, one, 0)
+
+    def whole(chunk, source, target, send, recv, peers=PEERS):
+        low = max(1, chunk * peers)
+        span = pl.ds(low, (chunk + 1) * peers - low)
         return pltpu.make_async_remote_copy(
             src_ref=source.at[span], dst_ref=target.at[span], send_sem=send,
             recv_sem=recv.at[chunk], device_id=device_at(1, 1), device_id_type=MESH,
         )
 
     for chunk in range(CHUNKS):
-        def fill(k, carry):
-            col = pl.ds(pl.multiple_of(k * TILE, TILE), TILE)
-            part = jnp.dot(
-                gates[chunk * ROWS:(chunk + 1) * ROWS, :], normed[:, col],
-                preferred_element_type=F32,
-            ).astype(BF)
-            sendbuf[chunk * PEERS:(chunk + 1) * PEERS, :, col] = part.reshape(PEERS, CAP, TILE)
-            return carry
-
-        lax.fori_loop(0, 4, fill, 0)
         send_all(chunk, sendbuf, recvbuf, dsend, drecv, 1)
     recvbuf[0] = sendbuf[0]
     for copy in fetched[9:]:
@@ -282,13 +273,21 @@
     for chunk in range(CHUNKS):
         whole(chunk, sendbuf, recvbuf, dsend, drecv).wait_recv()
         peers = slice(chunk * PEERS, (chunk + 1) * PEERS)
-        xs[...] = recvbuf[peers].reshape(ROWS, 2048)
+
+        def normalise(g, carry):
+            wide = recvbuf[pl.ds(chunk * PEERS + g * 4, 4)].reshape(16, 2048).astype(F32)
+            mean = jnp.sum(wide * wide, axis=1, keepdims=True) / 2048
+            normed = wide * lax.rsqrt(mean + 1e-06) * ffn_gain[...]
+            xs[pl.ds(pl.multiple_of(g * 16, 16), 16), :] = normed.astype(BF)
+            return carry
+
+        lax.fori_loop(0, ROWS // 16, normalise, 0)
 
         def up(j, carry):
             col = pl.ds(pl.multiple_of(j * TILE, TILE), TILE)
             gated_part = jnp.dot(xs[...], wg[:, col], preferred_element_type=F32)
             up_part = jnp.dot(xs[...], wu[:, col], preferred_element_type=F32)
-            hid[:, col] = (gated_part * jax.nn.sigmoid(gated_part) * up_part).astype(BF)
+            hid[:, col] = (gated_part * sigmoid(gated_part) * up_part).astype(BF)
             return carry
 
         lax.fori_loop(0, 1024 // TILE, up, 0)
@@ -302,32 +301,30 @@
         lax.fori_loop(0, 2048 // TILE, down, 0)
         if chunk == 0:
             yrecv[0] = ysend[0]
-        send_all(chunk, ysend, yrecv, rsend, rrecv, -1)
-
-    for chunk in range(CHUNKS):
-        whole(chunk, ysend, yrecv, rsend, rrecv).wait_recv()
-        peers = slice(chunk * PEERS, (chunk + 1) * PEERS)
-
-        def combine(j, carry):
-            col = pl.ds(pl.multiple_of(j * TILE, TILE), TILE)
-            got = yrecv[peers, :, col].reshape(ROWS, TILE)
-            both = jnp.dot(
-                wt[:, chunk * ROWS:(chunk + 1) * ROWS], got, preferred_element_type=F32
-            )
+        for part in range(BACK // CHUNKS):
+            send_all(chunk * BACK // CHUNKS + part, ysend, yrecv, rsend, rrecv, -1, N // BACK)
+
+    for chunk in range(BACK):
+        whole(chunk, ysend, yrecv, rsend, rrecv, N // BACK).wait_recv()
+        peers = slice(chunk * N // BACK, (chunk + 1) * N // BACK)
+        slots = slice(chunk * N // BACK * CAP, (chunk + 1) * N // BACK * CAP)
+
+        for j in range(2048 // TILE):
+            col = slice(j * TILE, (j + 1) * TILE)
+            got = yrecv[peers, :, col].reshape(N // BACK * CAP, TILE)
+            both = jnp.dot(wt[:, slots], got, preferred_element_type=F32)
             part = both[0:N] + both[N:2 * N]
             if chunk == 0:
                 acc[:, col] = part + stream[:, col].astype(F32)
-            elif chunk < CHUNKS - 1:
+            elif chunk < BACK - 1:
                 acc[:, col] = acc[:, col] + part
             else:
                 out_ref[:, col] = acc[:, col] + part
-            return carry
-
-        lax.fori_loop(0, 2048 // TILE, combine, 0)
 
     for chunk in range(CHUNKS):
         whole(chunk, sendbuf, recvbuf, dsend, drecv).wait_send()
-        whole(chunk, ysend, yrecv, rsend, rrecv).wait_send()
+    for chunk in range(BACK):
+        whole(chunk, ysend, yrecv, rsend, rrecv, N // BACK).wait_send()
     for copy in to_peer:
         copy.wait_send()
 
@@ -386,7 +383,6 @@
             pltpu.VMEM((12, 128, 128), F32),
             pltpu.VMEM((N, 1536), BF),
             pltpu.VMEM((N, 2048), BF),
-            pltpu.VMEM((N, 2048), BF),
             slots, slots, slots, slots,
             pltpu.VMEM((ROWS, 2048), BF),
             pltpu.VMEM((ROWS, 1024), BF),
@@ -394,7 +390,7 @@
             pltpu.VMEM((2 * N, CAP * N), BF),
             pltpu.VMEM((N, 2048), F32),
             dma((12,)), dma((3,)), dma((3,)), dma((2,)), dma((2,)), dma, dma((CHUNKS,)), dma,
-            dma((CHUNKS,)), pltpu.SemaphoreType.REGULAR, pltpu.SemaphoreType.REGULAR,
+            dma((BACK,)), pltpu.SemaphoreType.REGULAR, pltpu.SemaphoreType.REGULAR,
         ],
         compiler_params=pltpu.CompilerParams(
             collective_id=0, has_side_effects=True, vmem_limit_bytes=60 * 2**20

time: 67.1 us -> 64.8 us (0.966)
  Pallas kernels: 66.1 us -> 63.8 us
    pallas_call x1, Pallas kernels: 66.1 us -> 63.8 us  [per_device(): pl.pallas_call(layer_kernel, out_shape=pltpu.VMEM((N, 2048), F32), in_spe...]
where the time goes in v4:
time: 64.8 us; the launch traced here: 64.7 us
  Pallas kernels  63.8 us (98%)
  other arithmetic  0.86 us (1%)
    pallas_call x1, Pallas kernels, per_device(): pl.pallas_call(layer_kernel, out_shape=pltpu.VMEM((N, 2048), F32), in_spe...  63.8 us

profile of v4, /device:TPU:1, one launch (start us, length us, event | category | flops | bytes accessed | tf_op | source)
XLA Modules:
  0.0 64.7 jit_solution(13735715801108173037)
XLA Ops:
  0.0 63.8 %layer.1 = f32[128,2048]{1,0:T(8,128)S(1)} custom-call(bf16[128,2048]{1,0:T(8,128)(2,1)} %resid_hbm.1, bf16[256,768]{1,0:T(8,128)(2,1)} %value_hbm.1, bf16[256,768]{1,0:T(8,128)(2,1)} %gate_hbm.1, f32[31,768]{1,0:T(8,128)} %taps_hbm.1, f32[768]{0:T(1024)} %gain_hbm.1, bf16[1536,2048]{1,0:T(8,128)(2,1)} %ow_hbm.1, f32[1,2048]{1,0:T(1,128)} %bitcast.9, ...), custom_call_target="tpu_custom_call" | custom-call | tf_op jit(solution)/shard_map/layer/pallas_call | solution.py:358
  63.8 0.9 %convert_element_type.3 = bf16[128,2048]{1,0:T(8,128)(2,1)} convert(f32[128,2048]{1,0:T(8,128)S(1)} %layer.1) | non-fusion elementwise | flops 262144 | bytes 1572864 | tf_op jit(solution)/shard_map/convert_element_type | solution.py:403

commit v5 on v4

--- a/solution.py
+++ b/solution.py
@@ -22,7 +22,7 @@
 
 def offsets(i):
     a, b, c = i % 4, (i // 4) % 4, (i // 16) % 4
-    return a, (a + b) % 4, (a + b + c) % 4, i // 64
+    return a, (a + b) % 4, (a + b + c) % 4, (i // 64 + i) % 2
 
 
 def sigmoid(v):
@@ -82,8 +82,17 @@
             (ow_hbm, ow), (wg_hbm, wg), (wu_hbm, wu), (wd_hbm, wd),
         ])
     ]
-    for copy in fetched:
+    for copy in fetched[:9]:
         copy.start()
+    slot = lax.broadcasted_iota(jnp.int32, (CAP * N, N), 0)
+    i, r = slot // CAP, slot % CAP
+    dz, dy, dx, dc = offsets(i)
+    z, y, x = (sp // 16 + dz) % 4, ((sp // 4) % 4 + dy) % 4, (sp % 4 + dx) % 4
+    expert = ((z * 4 + y) * 4 + x) * 2 + (tp + dc) % 2
+    rows = lax.broadcasted_iota(jnp.int32, (N, N), 0)
+    cols = lax.broadcasted_iota(jnp.int32, (N, N), 1)
+    before = jnp.where(rows < cols, 1.0, 0.0).astype(BF)
+    rank_of_slot = r.astype(F32)
     for copy in fetched[:4]:
         copy.wait()
 
@@ -124,8 +133,6 @@
 
         lax.fori_loop(0, 6, one, 0)
 
-    place(tp * 6, lambda lanes: glu[pl.ds(own_rows, 144), lanes], taps_in, gain_in)
-    inner_blocks(tp * 6)
     expected = 13 + jnp.where(sp > 0, 1, 0) + jnp.where(sp < 63, 1, 0)
     pl.semaphore_wait(barrier, expected)
 
@@ -160,35 +167,29 @@
     ]
     for copy in to_peer:
         copy.start()
+    place(tp * 6, lambda lanes: glu[pl.ds(own_rows, 144), lanes], taps_in, gain_in)
+    inner_blocks(tp * 6)
     for copy in fetched[4:6]:
         copy.wait()
 
-    slot = lax.broadcasted_iota(jnp.int32, (CAP * N, N), 0)
-    i, r = slot // CAP, slot % CAP
-    dz, dy, dx, dc = offsets(i)
-    z, y, x = (sp // 16 + dz) % 4, ((sp // 4) % 4 + dy) % 4, (sp % 4 + dx) % 4
-    expert = ((z * 4 + y) * 4 + x) * 2 + (tp + dc) % 2
     first = ids[0:1, :] == expert
     second = ids[1:2, :] == expert
     named = jnp.where(first | second, 1.0, 0.0)
-    rows = lax.broadcasted_iota(jnp.int32, (N, N), 0)
-    cols = lax.broadcasted_iota(jnp.int32, (N, N), 1)
-    before = jnp.where(rows < cols, 1.0, 0.0).astype(BF)
     rank = jnp.dot(named.astype(BF), before, preferred_element_type=F32)
-    chosen = jnp.where(rank == r.astype(F32), named, 0.0)
+    chosen = jnp.where(rank == rank_of_slot, named, 0.0)
     gates[...] = chosen.astype(BF)
     weight = jnp.transpose(chosen * jnp.where(first, mix[0:1, :], mix[1:2, :]))
     high = weight.astype(BF)
     wt[0:N, :] = high
     wt[N:2 * N, :] = (weight - high.astype(F32)).astype(BF)
 
+    pl.semaphore_wait(y_ready, 3)
+    for step in (2, 3, 1):
+        signal(z_ready, device_in_line(step, 0, 0, 0))
     for copy in to_peer:
         copy.wait_recv()
     place((1 - tp) * 6, lambda lanes: other[:, lanes], taps_other, gain_other)
     inner_blocks((1 - tp) * 6)
-    pl.semaphore_wait(y_ready, 3)
-    for step in (2, 3, 1):
-        signal(z_ready, device_in_line(step, 0, 0, 0))
 
     def channel_norm(start, count):
         span = pl.ds(start, count)
@@ -266,6 +267,8 @@
 
     for chunk in range(CHUNKS):
         send_all(chunk, sendbuf, recvbuf, dsend, drecv, 1)
+    for copy in fetched[9:]:
+        copy.start()
     recvbuf[0] = sendbuf[0]
     for copy in fetched[9:]:
         copy.wait()

time: 64.8 us -> 64.5 us (level)
  no operation moved by 1% of the time
where the time goes in v5:
time: 64.5 us; the launch traced here: 64.4 us
  Pallas kernels  63.6 us (99%)
  other arithmetic  0.86 us (1%)
    pallas_call x1, Pallas kernels, per_device(): pl.pallas_call(layer_kernel, out_shape=pltpu.VMEM((N, 2048), F32), in_spe...  63.6 us

profile of v5, /device:TPU:1, one launch (start us, length us, event | category | flops | bytes accessed | tf_op | source)
XLA Modules:
  0.0 64.4 jit_solution(18057613441931114165)
XLA Ops:
  0.0 63.6 %layer.1 = f32[128,2048]{1,0:T(8,128)S(1)} custom-call(bf16[128,2048]{1,0:T(8,128)(2,1)} %resid_hbm.1, bf16[256,768]{1,0:T(8,128)(2,1)} %value_hbm.1, bf16[256,768]{1,0:T(8,128)(2,1)} %gate_hbm.1, f32[31,768]{1,0:T(8,128)} %taps_hbm.1, f32[768]{0:T(1024)} %gain_hbm.1, bf16[1536,2048]{1,0:T(8,128)(2,1)} %ow_hbm.1, f32[1,2048]{1,0:T(1,128)} %bitcast.9, ...), custom_call_target="tpu_custom_call" | custom-call | tf_op jit(solution)/shard_map/layer/pallas_call | solution.py:361
  63.6 0.9 %convert_element_type.3 = bf16[128,2048]{1,0:T(8,128)(2,1)} convert(f32[128,2048]{1,0:T(8,128)S(1)} %layer.1) | non-fusion elementwise | flops 262144 | bytes 1572864 | tf_op jit(solution)/shard_map/convert_element_type | solution.py:406

commit v6 on v5

--- a/solution.py
+++ b/solution.py
@@ -154,7 +154,7 @@
         to_previous.start()
 
     for step in (2, 3, 1):
-        signal(y_ready, device_in_line(0, step, 0, 0))
+        signal(z_ready, device_in_line(step, 0, 0, 0))
     peer_rows = pl.ds(pl.multiple_of(112 * (1 - tp), 16), 144)
     to_peer = [
         pltpu.make_async_remote_copy(
@@ -183,9 +183,9 @@
     wt[0:N, :] = high
     wt[N:2 * N, :] = (weight - high.astype(F32)).astype(BF)
 
-    pl.semaphore_wait(y_ready, 3)
+    pl.semaphore_wait(z_ready, 3)
     for step in (2, 3, 1):
-        signal(z_ready, device_in_line(step, 0, 0, 0))
+        signal(y_ready, device_in_line(0, step, 0, 0))
     for copy in to_peer:
         copy.wait_recv()
     place((1 - tp) * 6, lambda lanes: other[:, lanes], taps_other, gain_other)
@@ -245,7 +245,7 @@
             ).astype(BF)
             peers = slice(group * GATHER // CAP, (group + 1) * GATHER // CAP)
             sendbuf[peers, :, col] = part.reshape(GATHER // CAP, CAP, TILE)
-    pl.semaphore_wait(z_ready, 3)
+    pl.semaphore_wait(y_ready, 3)
 
     def send_all(chunk, source, target, send, recv, sign, peers=PEERS):
         def one(i, carry):

time: 64.5 us -> 64.6 us (level)
  no operation moved by 1% of the time
where the time goes in v6:
time: 64.6 us; the launch traced here: 64.5 us
  Pallas kernels  63.6 us (98%)
  other arithmetic  0.86 us (1%)
    pallas_call x1, Pallas kernels, per_device(): pl.pallas_call(layer_kernel, out_shape=pltpu.VMEM((N, 2048), F32), in_spe...  63.6 us

profile of v6, /device:TPU:1, one launch (start us, length us, event | category | flops | bytes accessed | tf_op | source)
XLA Modules:
  0.0 64.5 jit_solution(8335657612952534307)
XLA Ops:
  0.0 63.6 %layer.1 = f32[128,2048]{1,0:T(8,128)S(1)} custom-call(bf16[128,2048]{1,0:T(8,128)(2,1)} %resid_hbm.1, bf16[256,768]{1,0:T(8,128)(2,1)} %value_hbm.1, bf16[256,768]{1,0:T(8,128)(2,1)} %gate_hbm.1, f32[31,768]{1,0:T(8,128)} %taps_hbm.1, f32[768]{0:T(1024)} %gain_hbm.1, bf16[1536,2048]{1,0:T(8,128)(2,1)} %ow_hbm.1, f32[1,2048]{1,0:T(1,128)} %bitcast.9, ...), custom_call_target="tpu_custom_call" | custom-call | tf_op jit(solution)/shard_map/layer/pallas_call | solution.py:361
  63.6 0.9 %convert_element_type.3 = bf16[128,2048]{1,0:T(8,128)(2,1)} convert(f32[128,2048]{1,0:T(8,128)S(1)} %layer.1) | non-fusion elementwise | flops 262144 | bytes 1572864 | tf_op jit(solution)/shard_map/convert_element_type | solution.py:406
